TPU v7x, 512 devices: a whole 4x8x8 slice. The times are simulated.
512 devices in a mesh: sp: 64 (over z, y), tp: 8 (over x, core).
Axes of the slice: x: 4, y: 8, z: 8, core: 2. Of those that a mesh axis runs over, the one named last changes fastest.
Arguments:
- resid: bfloat16 [8192, 2048], P('sp', 'tp'), may hold values from -6 to 6
- qa_nope: bfloat16 [8192, 1024], P('sp', 'tp'), may hold values from -6 to 6
- qb_nope: bfloat16 [8192, 1024], P('sp', 'tp'), may hold values from -6 to 6
- qa_rope: bfloat16 [8192, 512], P('sp', 'tp'), may hold values from -360 to 360
- qb_rope: bfloat16 [8192, 256], P('sp', 'tp'), may hold values from -360 to 360
- latent: bfloat16 [8192, 256], P('sp'), may hold values from -6 to 6
- key_rope: bfloat16 [8192, 32], P('sp'), may hold values from -4 to 4
- lat_gain: float32 [256], replicated, may hold values from 0.1 to 1.9
- wa_key: bfloat16 [256, 1024], P(None, 'tp'), may hold values from -0.375 to 0.375
- wa_val: bfloat16 [256, 1024], P(None, 'tp'), may hold values from -0.75 to 0.75
- wb_key: bfloat16 [256, 1024], P(None, 'tp'), may hold values from -0.375 to 0.375
- wb_val: bfloat16 [256, 1024], P(None, 'tp'), may hold values from -0.75 to 0.75
- gain_a: float32 [1024], P('tp'), may hold values from 0.1 to 1.9
- gain_b: float32 [1024], P('tp'), may hold values from 0.1 to 1.9
- wa_out: bfloat16 [1024, 2048], P('tp'), may hold values from -0.125 to 0.125
- wb_out: bfloat16 [1024, 2048], P('tp'), may hold values from -0.125 to 0.125
- norm1_gain: float32 [2048], replicated, may hold values from 0.1 to 1.9
- ffn_gate: bfloat16 [2048, 5632], P('sp', 'tp'), may hold values from -0.125 to 0.125
- ffn_val: bfloat16 [2048, 5632], P('sp', 'tp'), may hold values from -0.125 to 0.125
- conv_gate: float32 [3, 5632], P(None, 'tp'), may hold values from -3 to 3
- conv_val: float32 [3, 5632], P(None, 'tp'), may hold values from -3 to 3
- ffn_down: bfloat16 [5632, 2048], P('tp'), may hold values from -0.078125 to 0.078125
- norm2_gain: float32 [2048], P('tp'), may hold values from 0.1 to 1.9
Outputs:
- layer_out: bfloat16 [8192, 2048], P('sp', 'tp')
All inputs are finite; a program needn't handle non-finite values.
Results may differ from a plain program's by a relative error of at most 0.017.
Values may be sent and summed in bfloat16 or wider, within the bound.
A program may use at most 128 MiB of HBM per device.

v0:
```python
import jax
import jax.numpy as jnp
from jax import lax
from jax.sharding import PartitionSpec as P

D = 2048
HA = 16
DA = 64
HB = 8
DB = 128
DR = 32
KC = 3


THETA = 10000.0
EPS_RMS = 1e-06
EPS_NORM = 1e-05
ALPHA = 2.0**0.25


def from_everyone(array, axis):
    count = lax.axis_size(axis)
    return lax.all_to_all(
        jnp.broadcast_to(array[None], (count, *array.shape)), axis, 0, 0, tiled=True
    )


def over_copies(array, axis):
    return from_everyone(array, axis).sum(axis=0)


def split_up(array, dim, count):
    shape = array.shape
    blocks = array.reshape(*shape[:dim], count, shape[dim] // count, *shape[dim + 1 :])
    return jnp.moveaxis(blocks, dim, 0)


def summed_on_arrival(array, axis, dim):
    count = lax.axis_size(axis)
    blocks = lax.all_to_all(split_up(array, dim, count), axis, 0, 0, tiled=True)
    return jnp.sum(blocks.astype(jnp.float32), axis=0)


def together(arrays, axis):
    ends = [0]
    for a in arrays:
        ends.append(ends[-1] + a.size)
    so_far = over_copies(jnp.concatenate([a.ravel() for a in arrays]), axis)
    return tuple((so_far[b:e].reshape(a.shape) for a, b, e in zip(arrays, ends, ends[1:])))


def laid_out(blocks, dim):
    blocks = jnp.moveaxis(blocks, 0, dim)
    shape = blocks.shape
    return blocks.reshape(*shape[:dim], shape[dim] * shape[dim + 1], *shape[dim + 2 :])


def gather_directly(array, axis, dim):
    return laid_out(from_everyone(array, axis), dim)


def side_by_side(arrays, axis, dim, along):
    both = jnp.concatenate(arrays, axis=along)
    filled, at, done = (lax.all_gather(both, axis, axis=dim, tiled=True), 0, [])
    for a in arrays:
        done.append(lax.slice_in_dim(filled, at, at + a.shape[along], axis=along))
        at += a.shape[along]
    return tuple(done)


def passed_along(value, axis, steps):
    count = lax.axis_size(axis)
    leading, last = (max(0, -steps), min(count, count - steps))
    return lax.ppermute(value, axis, [(source, source + steps) for source in range(leading, last)])


def rotary(values, positions):
    half = values.shape[-1] // 2
    freq = THETA ** (-jnp.arange(half, dtype=jnp.float32) * 2.0 / values.shape[-1])
    angle = positions.astype(jnp.float32)[:, None] * freq[None, :]
    if values.ndim == 3:
        angle = angle[:, None, :]
    cosine = jnp.cos(angle)
    sine = jnp.sin(angle)
    first = values[..., :half]
    second = values[..., half:]
    return jnp.concatenate(
        [first * cosine - second * sine, second * cosine + first * sine], axis=-1
    )


def rms_scale(values, gain):
    wide = values.astype(jnp.float32)
    return wide * lax.rsqrt(jnp.mean(wide * wide, axis=-1, keepdims=True) + EPS_RMS) * gain


def finish_norm(values, sums, gain, width):
    center = sums[0] / width
    spread = sums[1] / width - center * center
    return (values - center[:, None]) * lax.rsqrt(spread + EPS_NORM)[:, None] * gain


def start_carry(count, heads, width):
    return (
        jnp.full((heads, count), -1e30, jnp.float32),
        jnp.zeros((heads, count), jnp.float32),
        jnp.zeros((count, heads, width), jnp.float32),
    )


def divide_total(carry):
    mixed = carry[2] / jnp.transpose(carry[1])[:, :, None]
    return mixed.reshape(mixed.shape[0], mixed.shape[1] * mixed.shape[2])


def causal_taps(extended, taps, count):
    total = jnp.zeros((count, extended.shape[1]), jnp.float32)
    for tap in range(KC):
        total = total + taps[tap] * extended[tap : tap + count].astype(jnp.float32)
    return total


def shards(
    resid,
    qa_nope,
    qb_nope,
    qa_rope,
    qb_rope,
    latent,
    key_rope,
    lat_gain,
    wa_key,
    wa_val,
    wb_key,
    wb_val,
    gain_a,
    gain_b,
    wa_out,
    wb_out,
    norm1_gain,
    ffn_gate,
    ffn_val,
    conv_gate,
    conv_val,
    ffn_down,
    norm2_gain,
):
    tok_rows = resid.shape[0]
    positions = lax.axis_index("sp") * tok_rows + jnp.arange(tok_rows)
    heads_a = qa_nope.shape[1] // DA
    heads_b = qb_nope.shape[1] // DB
    lat_n = rms_scale(latent, lat_gain).astype(jnp.bfloat16)
    k_rot = rotary(key_rope.astype(jnp.float32), positions).astype(jnp.bfloat16)
    rot_a = rotary(qa_rope.astype(jnp.float32).reshape(tok_rows, heads_a, DR), positions).astype(
        jnp.bfloat16
    )
    rot_b = rotary(qb_rope.astype(jnp.float32).reshape(tok_rows, heads_b, DR), positions).astype(
        jnp.bfloat16
    )
    query_a = qa_nope.reshape(tok_rows, heads_a, DA)
    query_b = qb_nope.reshape(tok_rows, heads_b, DB)

    def absorb(carry, query, q_rot, keys, k_part, vals):
        width = query.shape[2]
        scale = (width + DR) ** (-0.5)
        count = keys.shape[0]
        scores = jnp.einsum("qhd,khd->hqk", query, keys, preferred_element_type=jnp.float32)
        scores = (
            scores + jnp.einsum("qhr,kr->hqk", q_rot, k_part, preferred_element_type=jnp.float32)
        ) * scale
        key_pos = jnp.arange(count)
        allowed = key_pos[None, :] <= positions[:, None]
        scores = jnp.where(allowed[None], scores, -1e30)
        top_old, total_old, running_old = carry
        top_new = jnp.maximum(top_old, jnp.max(scores, axis=-1))
        weights = jnp.exp(scores - top_new[:, :, None])
        total_new = jnp.sum(weights, axis=-1)
        update = jnp.einsum(
            "hqk,khd->qhd", weights.astype(jnp.bfloat16), vals, preferred_element_type=jnp.float32
        )
        return (top_new, total_new, update)

    def project(source, weight, heads, width):
        result = jnp.dot(source, weight, preferred_element_type=jnp.float32).astype(jnp.bfloat16)
        return result.reshape(source.shape[0], heads, width)

    empty = (start_carry(tok_rows, heads_a, DA), start_carry(tok_rows, heads_b, DB))
    pieces = (
        lax.all_gather(lat_n, "sp", axis=0, tiled=True),
        lax.all_gather(k_rot, "sp", axis=0, tiled=True),
    )
    first_group = absorb(
        empty[0],
        query_a,
        rot_a,
        project(pieces[0], wa_key, heads_a, DA),
        pieces[1],
        project(pieces[0], wa_val, heads_a, DA),
    )
    second_group = absorb(
        empty[1],
        query_b,
        rot_b,
        project(pieces[0], wb_key, heads_b, DB),
        pieces[1],
        project(pieces[0], wb_val, heads_b, DB),
    )
    raw_a = divide_total(first_group)
    raw_b = divide_total(second_group)
    local_energy = jnp.sum(raw_a * raw_a, axis=1) + jnp.sum(raw_b * raw_b, axis=1)
    energy = over_copies(local_energy, "tp")
    head_factor = lax.rsqrt(energy / (HA * DA + HB * DB) + EPS_RMS)[:, None]
    out_a = (raw_a * head_factor * gain_a).astype(jnp.bfloat16)
    out_b = (raw_b * head_factor * gain_b).astype(jnp.bfloat16)
    partial_value = jnp.dot(out_a, wa_out, preferred_element_type=jnp.float32) + jnp.dot(
        out_b, wb_out, preferred_element_type=jnp.float32
    )
    columns = resid.shape[1]
    mix_cols = summed_on_arrival(partial_value.astype(jnp.bfloat16), "tp", 1)
    pre_one = ALPHA * resid.astype(jnp.float32) + mix_cols
    sums_one = together((jnp.sum(pre_one, axis=1), jnp.sum(pre_one * pre_one, axis=1)), "tp")
    gain_cols = lax.dynamic_slice_in_dim(norm1_gain, lax.axis_index("tp") * columns, columns, 0)
    first_cols = finish_norm(pre_one, sums_one, gain_cols, D).astype(jnp.bfloat16)
    first_full = gather_directly(first_cols, "tp", 1)
    pieces = side_by_side((ffn_gate, ffn_val), "sp", 0, 1)
    count = pieces[0].shape[0]
    gate_sum = jnp.dot(first_full, pieces[0], preferred_element_type=jnp.float32)
    val_sum = jnp.dot(first_full, pieces[1], preferred_element_type=jnp.float32)
    gate_up = gate_sum.astype(jnp.bfloat16)
    val_up = val_sum.astype(jnp.bfloat16)
    rim_gate, rim_val = passed_along(
        (gate_up[tok_rows - (KC - 1) :], val_up[tok_rows - (KC - 1) :]), "sp", 1
    )
    gate_c = causal_taps(jnp.concatenate([rim_gate, gate_up], axis=0), conv_gate, tok_rows)
    val_c = causal_taps(jnp.concatenate([rim_val, val_up], axis=0), conv_val, tok_rows)
    hidden = (jax.nn.silu(gate_c) * val_c).astype(jnp.bfloat16)
    down = jnp.dot(hidden, ffn_down, preferred_element_type=jnp.float32)
    ff_cols = summed_on_arrival(down.astype(jnp.bfloat16), "tp", 1)
    pre_two = ALPHA * first_cols.astype(jnp.float32) + ff_cols
    sums_two = together((jnp.sum(pre_two, axis=1), jnp.sum(pre_two * pre_two, axis=1)), "tp")
    return finish_norm(pre_two, sums_two, norm2_gain, D).astype(jnp.bfloat16)


def solution(mesh):
    return jax.shard_map(
        shards,
        mesh=mesh,
        in_specs=(
            P("sp", "tp"),
            P("sp", "tp"),
            P("sp", "tp"),
            P("sp", "tp"),
            P("sp", "tp"),
            P("sp", None),
            P("sp", None),
            P(),
            P(None, "tp"),
            P(None, "tp"),
            P(None, "tp"),
            P(None, "tp"),
            P("tp"),
            P("tp"),
            P("tp", None),
            P("tp", None),
            P(),
            P("sp", "tp"),
            P("sp", "tp"),
            P(None, "tp"),
            P(None, "tp"),
            P("tp", None),
            P("tp"),
        ),
        out_specs=P("sp", "tp"),
        check_vma=False,
    )
```

profile of v0, /device:TPU:1, one launch (start us, length us, event | category | flops | bytes accessed | tf_op | source)
XLA Modules:
  0.0 240.8 jit_solution(9243384232271088843)
XLA Ops:
  6.5 1.1 fusion.57
  7.7 1.6 fusion.59
  9.3 1.5 pad_maximum_fusion.4
  13.4 48.3 %all_gather.10 = bf16[8192,32]{0,1:T(8,128)(2,1)S(1)} all-gather(bf16[128,32]{0,1:T(8,128)(2,1)S(1)} %pad_maximum_fusion.5), channel_id=1, replica_groups=mesh['sp'=64,'tp'=8] {'sp'}, dimensions={0}, use_global_device_ids=true | all-gather | bytes 532480 | tf_op jit(solution)/shard_map/all_gather | solution.py:190
  62.5 2.8 %convolution_bitcast_fusion.2 = f32[1,128,8192]{1,2,0:T(8,128)} fusion(bf16[8192,32]{0,1:T(8,128)(2,1)S(1)} %all_gather.10, bf16[128,16]{0,1:T(8,128)(2,1)S(1)} %get-tuple-element.18, bf16[128,16]{0,1:T(8,128)(2,1)S(1)} %get-tuple-element.17), kind=kOutput, calls=%fused_computation.5 | convolution fusion | flops 67125248 | bytes 4726784 | tf_op jit(solution)/shard_map/qhr,kr->hqk/dot_general | solution.py:169
  65.2 1.7 iota_compare_fusion.1
  66.9 31.7 %all-gather.3.cloned.1.call-done = bf16[8192,256]{1,0:T(8,128)(2,1)} async-done(((bf16[128,256]{1,0:T(8,128)(2,1)}), bf16[8192,256]{1,0:T(8,128)(2,1)}) %all-gather.3.cloned.1.call-update) | async-done | bytes 4194320 | tf_op jit(solution)/shard_map/all_gather | solution.py:189
  98.6 7.7 %fusion.88 = (f32[128]{0:T(128)S(1)}, f32[1,128,8192]{1,2,0:T(8,128)}) fusion(f32[1,128,8192]{1,2,0:T(8,128)} %convolution_bitcast_fusion.2, bf16[128,128]{1,0:T(8,128)(2,1)} %param.25, bf16[8192,256]{1,0:T(8,128)(2,1)} %all-gather.3.cloned.1.call-done, bf16[256,128]{1,0:T(8,128)(2,1)S(1)} %copy-done.9, s32[128]{0:T(128)} %copy-done.14), kind=kOutput, calls=%fused_computation.136 | convolution fusion | flops 811597696 | bytes 12682240 | tf_op jit(solution)/shard_map/qhd,khd->hqk/dot_general | solution.py:167
  106.3 3.7 %convolution_convert_fusion.2 = bf16[8192,128]{0,1:T(8,128)(2,1)S(1)} fusion(bf16[8192,256]{1,0:T(8,128)(2,1)} %all-gather.3.cloned.1.call-done, bf16[256,128]{1,0:T(8,128)(2,1)} %param.31), kind=kOutput, calls=%fused_computation.12 | convolution fusion | flops 537919488 | bytes 6356992 | tf_op jit(solution)/shard_map/dot_general | solution.py:184
  110.0 1.7 convolution_bitcast_fusion.1
  111.8 2.0 fusion.87
  113.9 1.1 fusion.11
  115.0 3.9 %copy-done.1 = bf16[8192,256]{1,0:T(8,128)(2,1)S(1)} copy-done((bf16[8192,256]{1,0:T(8,128)(2,1)S(1)}, bf16[8192,256]{1,0:T(8,128)(2,1)}, u32[]{:S(2)}) %copy-start.1) | copy-done | bytes 4194328
  119.0 2.8 %convolution_convert_fusion.3 = bf16[8192,128]{0,1:T(8,128)(2,1)} fusion(bf16[8192,256]{1,0:T(8,128)(2,1)S(1)} %copy-done.1, bf16[256,128]{1,0:T(8,128)(2,1)S(1)} %copy-done.10), kind=kOutput, calls=%fused_computation.13 | convolution fusion | flops 537919488 | bytes 6356992 | tf_op jit(solution)/shard_map/dot_general | solution.py:184
  121.8 1.1 fusion.6
  122.9 6.0 %multiply_reduce_fusion.2 = (f32[128]{0:T(128)S(1)}, f32[128,128]{0,1:T(8,128)S(1)}) fusion(f32[128]{0:T(128)S(1)} %fusion.11, f32[1,128,8192]{1,2,0:T(8,128)} %get-tuple-element.34, f32[128]{0:T(128)S(1)} %broadcast_maximum_fusion.1, bf16[8192,256]{1,0:T(8,128)(2,1)} %all-gather.3.cloned.1.call-done, bf16[256,128]{1,0:T(8,128)(2,1)S(1)} %copy-done.11), kind=kOutput, calls=%fused_computation.80 | convolution fusion | flops 808501120 | bytes 8521216 | tf_op jit(solution)/shard_map/hqk,khd->qhd/dot_general | solution.py:178
  128.9 5.7 %multiply_reduce_fusion.3 = (f32[128]{0:T(128)S(1)}, f32[128,2,64]{0,2,1:T(8,128)S(1)}) fusion(f32[128,2]{0,1:T(2,128)S(1)} %bitcast.121, bf16[8192,2,64]{0,2,1:T(8,128)(2,1)} %bitcast.110, f32[2,128,8192]{1,2,0:T(8,128)} %copy-done.2, f32[2,128]{1,0:T(2,128)S(1)} %broadcast_maximum_fusion), kind=kOutput, calls=%fused_computation.81 | convolution fusion | flops 272678784 | bytes 10553856 | tf_op jit(solution)/shard_map/hqk,khd->qhd/dot_general | solution.py:178
  134.6 13.5 %all_to_all.33 = f32[8,1,128]{2,1,0:T(1,128)S(1)} all-to-all(f32[8,1,128]{2,1,0:T(1,128)S(1)} %broadcast_in_dim.33), channel_id=1, replica_groups=mesh['sp'=64,'tp'=8] {'tp'}, dimensions={0} | all-to-all | bytes 8192 | tf_op jit(solution)/shard_map/all_to_all | solution.py:23
  148.5 1.5 fusion.17
  150.0 12.5 %all_to_all.34 = bf16[8,128,256]{2,1,0:T(8,128)(2,1)S(1)} all-to-all(bf16[8,128,256]{2,1,0:T(8,128)(2,1)S(1)} %bitcast.112), channel_id=1, replica_groups=mesh['sp'=64,'tp'=8] {'tp'}, dimensions={0} | all-to-all | bytes 1048576 | tf_op jit(solution)/shard_map/all_to_all | solution.py:40
  163.3 4.2 %all-to-all-start.2 = ((f32[8,1,256]{2,1,0:T(1,128)}), f32[8,1,256]{2,1,0:T(1,128)S(1)}, u32[]{:S(2)}, u32[]{:S(2)}) async-start(f32[8,1,256]{2,1,0:T(1,128)} %broadcast_in_dim.34), calls=%async_computation.2 | async-start | bytes 16384 | tf_op jit(solution)/shard_map/all_to_all | solution.py:23
  168.3 4.0 %all-to-all-done.2 = f32[8,1,256]{2,1,0:T(1,128)S(1)} async-done(((f32[8,1,256]{2,1,0:T(1,128)}), f32[8,1,256]{2,1,0:T(1,128)S(1)}, u32[]{:S(2)}, u32[]{:S(2)}) %all-to-all-start.2) | async-done | bytes 8224 | tf_op jit(solution)/shard_map/all_to_all | solution.py:23
  172.6 13.0 %all_to_all.35 = bf16[8,128,256]{1,2,0:T(8,128)(2,1)} all-to-all(bf16[8,128,256]{1,2,0:T(8,128)(2,1)S(1)} %broadcast_in_dim.35), channel_id=1, replica_groups=mesh['sp'=64,'tp'=8] {'tp'}, dimensions={0} | all-to-all | bytes 1048576 | tf_op jit(solution)/shard_map/all_to_all | solution.py:23
  185.6 2.9 %all-gather.5.cloned.1.call-done = bf16[2048,1408]{1,0:T(8,128)(2,1)} async-done(((bf16[32,1408]{1,0:T(8,128)(2,1)}), bf16[2048,1408]{1,0:T(8,128)(2,1)}) %all-gather.5.cloned.1.call-update) | async-done | bytes 5767184 | tf_op jit(solution)/shard_map/all_gather | solution.py:64
  188.5 3.4 %fusion.22 = bf16[128,704]{0,1:T(8,128)(2,1)S(1)} fusion(bf16[128,2048]{0,1:T(8,128)(2,1)} %bitcast.115, bf16[2048,1408]{1,0:T(8,128)(2,1)} %all-gather.5.cloned.1.call-done), kind=kOutput, calls=%fused_computation.34 | convolution fusion | flops 369188864 | bytes 3850240 | tf_op jit(solution)/shard_map/dot_general | solution.py:227
  192.0 2.7 %collective-permute-start = (bf16[2,704]{0,1:T(8,128)(2,1)S(1)}, bf16[2,704]{0,1:T(8,128)(2,1)S(1)}, u32[]{:S(2)}, u32[]{:S(2)}) collective-permute-start(bf16[2,704]{0,1:T(8,128)(2,1)S(1)} %slice.103), channel_id=1, source_target_pairs={{0,8},{8,16},{16,24},{24,32},{32,40},{40,48},{48,56},{56,64},{64,7... | collective-permute-start | bytes 8456 | tf_op jit(solution)/shard_map/ppermute | solution.py:74
  194.7 4.6 %fusion.25 = bf16[128,704]{0,1:T(8,128)(2,1)S(1)} fusion(bf16[128,2048]{0,1:T(8,128)(2,1)S(1)} %bitcast.116, bf16[2048,1408]{1,0:T(8,128)(2,1)} %all-gather.5.cloned.1.call-done), kind=kOutput, calls=%fused_computation.35 | convolution fusion | flops 369188864 | bytes 3850240 | tf_op jit(solution)/shard_map/dot_general | solution.py:228
  199.4 3.5 %collective-permute-start.1 = (bf16[2,704]{0,1:T(8,128)(2,1)S(1)}, bf16[2,704]{0,1:T(8,128)(2,1)S(1)}, u32[]{:S(2)}, u32[]{:S(2)}) collective-permute-start(bf16[2,704]{0,1:T(8,128)(2,1)S(1)} %slice.107), channel_id=1, source_target_pairs={{0,8},{8,16},{16,24},{24,32},{32,40},{40,48},{48,56},{56,64},{64,7... | collective-permute-start | bytes 8456 | tf_op jit(solution)/shard_map/ppermute | solution.py:74
  203.0 2.3 collective-permute-done.1
  205.3 1.5 convolution_convert_fusion.4
  206.9 18.0 %all_to_all.36 = bf16[8,128,256]{2,1,0:T(8,128)(2,1)S(1)} all-to-all(bf16[8,128,256]{2,1,0:T(8,128)(2,1)S(1)} %bitcast.113), channel_id=1, replica_groups=mesh['sp'=64,'tp'=8] {'tp'}, dimensions={0} | all-to-all | bytes 1048576 | tf_op jit(solution)/shard_map/all_to_all | solution.py:40
  225.1 8.0 %all_to_all.37 = f32[8,1,256]{2,1,0:T(1,128)S(1)} all-to-all(f32[8,1,256]{2,1,0:T(1,128)S(1)} %broadcast_in_dim.36), channel_id=1, replica_groups=mesh['sp'=64,'tp'=8] {'tp'}, dimensions={0} | all-to-all | bytes 16384 | tf_op jit(solution)/shard_map/all_to_all | solution.py:23
  (80 shorter events, 7.3 us)
Async XLA Ops:
  6.5 198.8 %copy-start = (bf16[704,2048]{1,0:T(8,128)(2,1)S(1)}, bf16[704,2048]{1,0:T(8,128)(2,1)}, u32[]{:S(2)}) copy-start(bf16[704,2048]{1,0:T(8,128)(2,1)} %param.44) | copy-start | bytes 8650756
  6.5 92.1 %copy-start.9 = (bf16[256,128]{1,0:T(8,128)(2,1)S(1)}, bf16[256,128]{1,0:T(8,128)(2,1)}, u32[]{:S(2)}) copy-start(bf16[256,128]{1,0:T(8,128)(2,1)} %param.33) | copy-start | bytes 196612
  6.5 92.1 %all-gather.3.cloned.1.call-start = ((), (), s32[]{:S(2)}) async-start(), calls=%async_computation.6 | async-start | bytes 4259840 | tf_op jit(solution)/shard_map/all_gather | solution.py:189
  9.3 179.2 %all-gather.5.cloned.1.call-start = ((), (), s32[]{:S(2)}) async-start(), calls=%async_computation.7 | async-start | bytes 5857280 | tf_op jit(solution)/shard_map/all_gather | solution.py:64
  13.2 52.0 %copy-start.14 = (s32[128]{0:T(128)}, s32[128]{0:T(128)S(1)}, u32[]{:S(2)}) copy-start(s32[128]{0:T(128)S(1)} %iota_add_fusion) | copy-start | bytes 1540
  110.0 1.8 copy-start.4
  111.7 2.2 copy-start.3
  111.7 3.3 %copy-start.10 = (bf16[256,128]{1,0:T(8,128)(2,1)S(1)}, bf16[256,128]{1,0:T(8,128)(2,1)}, u32[]{:S(2)}) copy-start(bf16[256,128]{1,0:T(8,128)(2,1)} %param.32) | copy-start | bytes 196612
  113.7 8.1 %copy-start.2 = (f32[2,128,8192]{1,2,0:T(8,128)}, f32[2,128,8192]{1,2,0:T(8,128)S(1)}, u32[]{:S(2)}) copy-start(f32[2,128,8192]{1,2,0:T(8,128)S(1)} %get-tuple-element.30) | copy-start | bytes 25165828
  113.7 5.2 %copy-start.1 = (bf16[8192,256]{1,0:T(8,128)(2,1)S(1)}, bf16[8192,256]{1,0:T(8,128)(2,1)}, u32[]{:S(2)}) copy-start(bf16[8192,256]{1,0:T(8,128)(2,1)} %all-gather.3.cloned.1.call-done) | copy-start | bytes 12582916
  121.8 1.1 copy-start.11
  128.9 19.2 %copy-start.16 = (f32[128]{0:T(128)S(1)}, f32[128]{0:T(128)}, u32[]{:S(2)}) copy-start(f32[128]{0:T(128)} %param.35) | copy-start | bytes 1540
  128.9 19.3 %copy-start.5 = (bf16[128,2048]{1,0:T(8,128)(2,1)S(1)}, bf16[128,2048]{1,0:T(8,128)(2,1)}, u32[]{:S(2)}) copy-start(bf16[128,2048]{1,0:T(8,128)(2,1)} %param.37) | copy-start | bytes 1572868
  148.1 14.5 %copy-start.7 = (bf16[128,256]{1,0:T(8,128)(2,1)S(1)}, bf16[128,256]{1,0:T(8,128)(2,1)}, u32[]{:S(2)}) copy-start(bf16[128,256]{1,0:T(8,128)(2,1)} %param.23) | copy-start | bytes 196612
  148.2 24.1 %copy-start.8 = (bf16[128,256]{1,0:T(8,128)(2,1)S(1)}, bf16[128,256]{1,0:T(8,128)(2,1)}, u32[]{:S(2)}) copy-start(bf16[128,256]{1,0:T(8,128)(2,1)} %param.23) | copy-start | bytes 196612
  163.3 9.0 %all-to-all-start.2 = ((f32[8,1,256]{2,1,0:T(1,128)}), f32[8,1,256]{2,1,0:T(1,128)S(1)}, u32[]{:S(2)}, u32[]{:S(2)}) async-start(f32[8,1,256]{2,1,0:T(1,128)} %broadcast_in_dim.34), calls=%async_computation.2 | async-start | bytes 16384 | tf_op jit(solution)/shard_map/all_to_all | solution.py:23
  188.5 6.2 %copy-start.6 = (bf16[8,128,256]{1,2,0:T(8,128)(2,1)S(1)}, bf16[8,128,256]{1,2,0:T(8,128)(2,1)}, u32[]{:S(2)}) copy-start(bf16[8,128,256]{1,2,0:T(8,128)(2,1)} %all_to_all.35) | copy-start | bytes 1572868
  188.5 14.4 %copy-start.12 = (f32[3,704]{1,0:T(4,128)S(1)}, f32[3,704]{1,0:T(4,128)}, u32[]{:S(2)}) copy-start(f32[3,704]{1,0:T(4,128)} %param.43) | copy-start | bytes 25348
  188.5 14.4 %copy-start.13 = (f32[3,704]{1,0:T(4,128)S(1)}, f32[3,704]{1,0:T(4,128)}, u32[]{:S(2)}) copy-start(f32[3,704]{1,0:T(4,128)} %param.42) | copy-start | bytes 25348
  192.0 11.0 %collective-permute-start = (bf16[2,704]{0,1:T(8,128)(2,1)S(1)}, bf16[2,704]{0,1:T(8,128)(2,1)S(1)}, u32[]{:S(2)}, u32[]{:S(2)}) collective-permute-start(bf16[2,704]{0,1:T(8,128)(2,1)S(1)} %slice.103), channel_id=1, source_target_pairs={{0,8},{8,16},{16,24},{24,32},{32,40},{40,48},{48,56},{56,64},{64,7... | collective-permute-start | bytes 8456 | tf_op jit(solution)/shard_map/ppermute | solution.py:74
  199.4 5.9 %collective-permute-start.1 = (bf16[2,704]{0,1:T(8,128)(2,1)S(1)}, bf16[2,704]{0,1:T(8,128)(2,1)S(1)}, u32[]{:S(2)}, u32[]{:S(2)}) collective-permute-start(bf16[2,704]{0,1:T(8,128)(2,1)S(1)} %slice.107), channel_id=1, source_target_pairs={{0,8},{8,16},{16,24},{24,32},{32,40},{40,48},{48,56},{56,64},{64,7... | collective-permute-start | bytes 8456 | tf_op jit(solution)/shard_map/ppermute | solution.py:74
  205.3 27.8 %copy-start.15 = (f32[256]{0:T(256)S(1)}, f32[256]{0:T(256)}, u32[]{:S(2)}) copy-start(f32[256]{0:T(256)} %param.45) | copy-start | bytes 3076
Sparse Core Ops, SparseCore 0:
  10.4 88.1 all-gather.2
  101.6 86.8 all-gather.4
where the time goes:
time: 242 us; the launch traced here: 241 us
  blocking collectives  113 us (47%)
  matrix products  43.5 us (18%)
  waiting for transfers between devices  40.9 us (17%)
  between operations  13.8 us (6%)
  other arithmetic  11.9 us (5%)
  starting transfers between devices  10.4 us (4%)
  local copies, waits for them, and re-layouts  6.94 us (3%)
    all_gather x1, blocking collectives, shards(): lax.all_gather(k_rot, 'sp', axis=0, tiled=True)  48.3 us
    all_to_all x3, blocking collectives, from_everyone(): lax.all_to_all(jnp.broadcast_to(array[None], (count, *array.shape)), axis...  34.5 us
    all_gather x1, waiting for transfers between devices, shards(): lax.all_gather(lat_n, 'sp', axis=0, tiled=True)  31.7 us
    all_to_all x2, blocking collectives, summed_on_arrival(): blocks = lax.all_to_all(split_up(array, dim, count), axis, 0, 0, tiled=True)  30.5 us
    dot_general x2, matrix products, absorb(): jnp.einsum('hqk,khd->qhd', weights.astype(jnp.bfloat16), vals, preferred_...  11.6 us
    dot_general x2, matrix products, absorb(): jnp.einsum('qhd,khd->hqk', query, keys, preferred_element_type=jnp.float32)  9.42 us
    dot_general x2, matrix products, project(): jnp.dot(source, weight, preferred_element_type=jnp.float32)  6.49 us
    ppermute x2, starting transfers between devices, passed_along(): lax.ppermute(value, axis, [(source, source + steps) for source in range(l...  6.16 us
  transfers between devices with their start and end apart: 5, of which 4 were waited for; matrix products, arithmetic and copies ran while one was open for 21% of the time, Pallas kernels for 0%

commit v1 on v0

v1 whole, which is shorter than its diff:
```python
import jax
import jax.numpy as jnp
from jax import lax
from jax.experimental import pallas as pl
from jax.experimental.pallas import tpu as pltpu
from jax.sharding import PartitionSpec as P

D = 2048
HA = 16
DA = 64
HB = 8
DB = 128
DR = 32
LAT = 256
KC = 3
ROWS = 128
COLS = 256
UNITS = 704
MAIN = 640
HALO = 16
N = 8

THETA = 10000.0
EPS_RMS = 1e-06
EPS_NORM = 1e-05
ALPHA = 2.0**0.25
LOG2E = 1.4426950408889634
LOW = -1e30
MESH = pl.DeviceIdType.MESH
F32 = jnp.float32
BF16 = jnp.bfloat16


def dot(a, b):
    return jnp.dot(a, b, preferred_element_type=F32)


def dot_t(a, b):
    return lax.dot_general(a, b, (((1,), (1,)), ((), ())), preferred_element_type=F32)


def wrap(v):
    return lax.rem(v, N)


def kernel(
    cosine,
    sine,
    resid,
    qa_nope,
    qb_nope,
    qa_rope,
    qb_rope,
    latent,
    key_rope,
    lat_gain,
    wa_key,
    wa_val,
    wb_key,
    wb_val,
    gain_a,
    gain_b,
    wa_out,
    wb_out,
    norm1_gain,
    ffn_gate,
    ffn_val,
    conv_gate,
    conv_val,
    ffn_down,
    norm2_gain,
    out,
    lat,
    wgt,
    q_lat,
    q_rot,
    acc,
    top,
    total,
    w_out,
    w_down,
    mix_out,
    mix_in,
    energy,
    pre,
    first,
    first_own,
    up,
    hidden,
    down_out,
    down_in,
    stats,
    local_sem,
    l1s,
    l1r,
    w1s,
    w1r,
    l2s,
    l2r,
    dds,
    ddr,
    w2s,
    w2r,
    mxs,
    mxr,
    ens,
    enr,
    prs,
    prr,
    hls,
    hlr,
    dns,
    dnr,
    sts,
    srr,
):
    sp = lax.axis_index("sp")
    tp = lax.axis_index("tp")
    core = lax.rem(tp, 2)
    z = lax.div(sp, N)
    y = lax.rem(sp, N)
    alpha = y + core * (z - y)
    beta = z + core * (y - z)
    sa = 1 + 7 * core
    sb = 8 - 7 * core
    partner = (sp, tp + 1 - 2 * core)
    nxt = (lax.rem(sp + 1, N * N), tp)
    prv = (lax.rem(sp + N * N - 1, N * N), tp)

    def along_a(k):
        return (wrap(alpha + k) * sa + beta * sb, tp)

    def along_b(k):
        return (alpha * sa + wrap(beta + k) * sb, tp)

    def along_tp(k):
        return (sp, wrap(tp + k))

    def remote(src, dst, send, recv, device):
        return pltpu.make_async_remote_copy(
            src_ref=src, dst_ref=dst, send_sem=send, recv_sem=recv, device_id=device, device_id_type=MESH
        )

    pending = []

    def send(src, dst, ssem, rsem, device):
        copy = remote(src, dst, ssem, rsem, device)
        copy.start()
        pending.append(copy)

    def arrived(ref, rsem):
        remote(ref, ref, l1s.at[0], rsem, partner).wait_recv()

    barrier = pltpu.get_barrier_semaphore()
    peers = [along_a(k) for k in range(1, N)] + [along_b(1), along_b(N - 1)]
    peers += [along_tp(k) for k in range(1, N)] + [nxt, prv]
    for device in peers:
        pl.semaphore_signal(barrier, inc=1, device_id=device, device_id_type=MESH)

    local = [
        pltpu.make_async_copy(wa_out, w_out.at[0:128], local_sem.at[0]),
        pltpu.make_async_copy(wb_out, w_out.at[128:256], local_sem.at[1]),
        pltpu.make_async_copy(ffn_down, w_down, local_sem.at[2]),
    ]
    for copy in local:
        copy.start()

    half = pl.ds(pl.multiple_of(core * 64, 64), 64)
    wide = latent[half, :].astype(F32)
    wide = wide * lax.rsqrt(jnp.mean(wide * wide, axis=1, keepdims=True) + EPS_RMS) * lat_gain[...]
    lat_n = wide.astype(BF16)

    def rotated(v, c, s):
        return v * c + jnp.concatenate([v[:, DR // 2 :], v[:, : DR // 2]], axis=1) * s

    k_rot = rotated(key_rope[half, :].astype(F32), cosine[half, :], sine[half, :])
    k_wide = jnp.concatenate([k_rot, jnp.zeros((64, 128 - DR), F32)], axis=1)
    k_wide = jnp.concatenate([k_wide, jnp.zeros((64, 128), F32)], axis=0)
    k_t = k_wide.T
    k_packed = jnp.concatenate([k_t[0:16, 0:64], k_t[16:32, 0:64]], axis=1)
    lat[core, beta, alpha, 0:64, :] = lat_n[:, :128]
    lat[core, beta, alpha, 64:128, :] = lat_n[:, 128:]
    lat[core, beta, alpha, 128:144, :] = k_packed.astype(BF16)
    wgt[beta, alpha, :, 0:MAIN] = ffn_gate[:, :MAIN]
    wgt[beta, alpha, :, MAIN : 2 * MAIN] = ffn_val[:, :MAIN]
    wgt[beta, alpha, :, 2 * MAIN :] = jnp.concatenate(
        [ffn_gate[:, MAIN:].astype(F32), ffn_val[:, MAIN:].astype(F32)], axis=1
    ).astype(BF16)

    pl.semaphore_wait(barrier, len(peers))

    mine = lat.at[core, beta, alpha]
    for k in (4, 3, 5, 2, 6, 1, 7):
        send(mine, mine, l1s.at[k - 1], l1r.at[alpha], along_a(k))

    def weight_step(step, forward, backward):
        if forward:
            block = wgt.at[beta, wrap(alpha + N - step)]
            if step:
                arrived(block, w1r.at[wrap(alpha + N - step)])
            send(block, block, w1s.at[step], w1r.at[wrap(alpha + N - step)], along_a(1))
        if backward:
            block = wgt.at[beta, wrap(alpha + step)]
            if step:
                arrived(block, w1r.at[wrap(alpha + step)])
            send(block, block, w1s.at[4 + step], w1r.at[wrap(alpha + step)], along_a(N - 1))

    weight_step(0, True, True)

    q_scale_a = (DA + DR) ** (-0.5) * LOG2E
    q_scale_b = (DB + DR) ** (-0.5) * LOG2E
    for h in range(2):
        part = dot_t(qa_nope[:, h * DA : (h + 1) * DA], wa_key[:, h * DA : (h + 1) * DA])
        q_lat[h * ROWS : (h + 1) * ROWS, :] = (part * q_scale_a).astype(BF16)
        turned = rotated(qa_rope[:, h * DR : (h + 1) * DR].astype(F32), cosine[...], sine[...])
        q_rot[h * ROWS : (h + 1) * ROWS, :] = (turned * q_scale_a).astype(BF16)
    part = dot_t(qb_nope[...], wb_key[...])
    q_lat[2 * ROWS :, :] = (part * q_scale_b).astype(BF16)
    turned = rotated(qb_rope[...].astype(F32), cosine[...], sine[...])
    q_rot[2 * ROWS :, :] = (turned * q_scale_b).astype(BF16)
    acc[...] = jnp.zeros_like(acc)
    top[...] = jnp.full_like(top, LOW)
    total[...] = jnp.zeros_like(total)

    def lat_piece(b, p):
        return lat.at[core, b, pl.ds(4 * p, 4)]

    def lat_pass(d, p, forward, backward):
        for go, b, k, base in (
            (forward, wrap(beta + N - d), 1, 0),
            (backward, wrap(beta + d), N - 1, 7),
        ):
            if go:
                if d:
                    arrived(lat_piece(b, p), l2r.at[2 * b + p])
                at = base + (2 * d + p if d < 3 else 6)
                send(lat_piece(b, p), lat_piece(b, p), l2s.at[at], l2r.at[2 * b + p], along_b(k))

    def hand_over(b):
        send(lat.at[core, b], lat.at[core, b], dds.at[b], ddr.at[b], partner)

    def wgt_piece(b, p):
        return wgt.at[b, pl.ds(2 * p, 2)]

    def wgt_pass(d, p, forward=True, backward=True):
        for go, b, k, base in (
            (forward, wrap(beta + N - d), 1, 0),
            (backward, wrap(beta + d), N - 1, 14),
        ):
            if go:
                if d:
                    arrived(wgt_piece(b, p), w2r.at[4 * b + p])
                at = base + 4 * d + (p if d < 3 or k == 1 else p - 2)
                send(wgt_piece(b, p), wgt_piece(b, p), w2s.at[at], w2r.at[4 * b + p], along_b(k))

    for k in range(1, N):
        block = lat.at[core, beta, wrap(alpha + k)]
        arrived(block, l1r.at[wrap(alpha + k)])
    lat_pass(0, 0, True, True)
    lat_pass(0, 1, True, True)
    hand_over(beta)
    weight_step(1, True, True)
    weight_step(2, True, True)
    lat_pass(1, 0, True, True)
    weight_step(3, True, False)
    lat_pass(1, 1, True, True)
    hand_over(wrap(beta + N - 1))
    hand_over(wrap(beta + 1))
    lat_pass(2, 0, True, True)
    for k in (3, 4):
        a = wrap(alpha + k)
        arrived(wgt.at[beta, a], w1r.at[a])
    wgt_pass(0, 0)
    lat_pass(2, 1, True, True)
    hand_over(wrap(beta + N - 2))
    hand_over(wrap(beta + 2))
    wgt_pass(0, 1)
    lat_pass(3, 0, True, False)
    lat_pass(3, 1, False, True)
    wgt_pass(0, 2)
    wgt_pass(0, 3)
    for b, p in ((wrap(beta + N - 3), 1), (wrap(beta + 3), 0)):
        arrived(lat_piece(b, p), l2r.at[2 * b + p])
    hand_over(wrap(beta + N - 3))
    hand_over(wrap(beta + 3))
    b = wrap(beta + 4)
    arrived(lat_piece(b, 0), l2r.at[2 * b])
    arrived(lat_piece(b, 1), l2r.at[2 * b + 1])
    hand_over(b)

    def offset(i):
        steps = lax.div(i + 1, 2)
        return wrap(N + steps * (1 - 2 * lax.rem(i, 2)))

    def attend(i):
        b0 = wrap(z + offset(i))
        b1 = wrap(y + offset(i))
        theirs = b1 + core * (b0 - b1)
        arrived(lat.at[1 - core, theirs], ddr.at[theirs])
        left, right, roped = [], [], []
        for half_of, b in ((0, b0), (1, b1)):
            left.append(lat[half_of, b, :, 0:64, :].reshape(512, 128))
            right.append(lat[half_of, b, :, 64:128, :].reshape(512, 128))
            x = lat[half_of, b, :, 128:144, :]
            upper = [jnp.concatenate([x[a][:, :64], x[a + 1][:, :64]], axis=1) for a in range(0, N, 2)]
            lower = [jnp.concatenate([x[a][:, 64:], x[a + 1][:, 64:]], axis=1) for a in range(0, N, 2)]
            roped.append(
                jnp.concatenate(
                    [jnp.concatenate(upper, axis=1), jnp.concatenate(lower, axis=1)], axis=0
                )
            )
        keys = jnp.concatenate(
            [jnp.concatenate(left, axis=0), jnp.concatenate(right, axis=0)], axis=1
        )
        ropes = jnp.concatenate(roped, axis=1)
        scores = dot_t(q_lat[...], keys) + dot(q_rot[...], ropes)
        j = lax.broadcasted_iota(jnp.int32, (1, 1024), 1)
        a = lax.shift_right_logical(lax.bitwise_and(j, 511), 6)
        r = lax.bitwise_and(j, 63)
        spots = jnp.where(j < 512, b0 * 1024 + a * 128 + r, a * 1024 + b1 * 128 + 64 + r)
        rows = lax.broadcasted_iota(jnp.int32, (3 * ROWS, 1), 0)
        rows = sp * ROWS + lax.bitwise_and(rows, ROWS - 1)
        scores = jnp.where(spots <= rows, scores, LOW)
        old = top[:, 0:1]
        new = jnp.maximum(old, jnp.max(scores, axis=1, keepdims=True))
        weights = jnp.exp2(scores - new)
        shrink = jnp.exp2(old - new)
        total[...] = total[...] * shrink + jnp.sum(weights, axis=1, keepdims=True)
        acc[...] = acc[...] * shrink + dot(weights.astype(BF16), keys)
        top[...] = jnp.broadcast_to(new, top.shape)

    def attend_two(e):
        def body(i, carry):
            attend(i)
            return carry

        lax.fori_loop(2 * e, 2 * e + 2, body, 0)

    for e in range(4):
        attend_two(e)
        wgt_pass(1, e)

    normed = (acc[...] / total[:, 0:1]).astype(BF16)
    raw_a = jnp.concatenate(
        [dot(normed[h * ROWS : (h + 1) * ROWS], wa_val[:, h * DA : (h + 1) * DA]) for h in range(2)], axis=1
    )
    raw_b = dot(normed[2 * ROWS :], wb_val[...])
    power = jnp.sum(raw_a * raw_a, axis=1, keepdims=True) + jnp.sum(raw_b * raw_b, axis=1, keepdims=True)
    energy[tp] = jnp.broadcast_to(power, (ROWS, ROWS)).T[0:8]
    gained = jnp.concatenate([raw_a * gain_a[...], raw_b * gain_b[...]], axis=1).astype(BF16)
    local[0].wait()
    local[1].wait()

    def of_tp(t):
        return pl.ds(pl.multiple_of(t * COLS, COLS), COLS)

    order = (4, 5, 3, 2, 6, 7, 1)
    for k in order:
        t = wrap(tp + k)
        mix_out[t] = dot(gained, w_out[:, of_tp(t)]).astype(BF16)
        send(mix_out.at[t], mix_in.at[tp], mxs.at[k], mxr.at[tp], along_tp(k))
        send(energy.at[tp], energy.at[tp], ens.at[k], enr.at[tp], along_tp(k))
    mix = dot(gained, w_out[:, of_tp(tp)])
    wgt_pass(2, 0)
    wgt_pass(2, 1)
    for k in order:
        t = wrap(tp + k)
        arrived(mix_in.at[t], mxr.at[t])
        arrived(energy.at[t], enr.at[t])
        mix = mix + mix_in[t].astype(F32)
    power = energy[0]
    for t in range(1, N):
        power = power + energy[t]
    factor = lax.rsqrt(power[0:1] / (HA * DA + HB * DB) + EPS_RMS)
    factor = jnp.broadcast_to(factor, (ROWS, ROWS)).T[:, 0:1]
    pre[tp] = (ALPHA * resid[...].astype(F32) + mix * factor).astype(BF16)
    for k in order:
        send(pre.at[tp], pre.at[tp], prs.at[k], prr.at[tp], along_tp(k))
    wgt_pass(2, 2)
    wgt_pass(2, 3)
    wgt_pass(3, 0, True, False)
    wgt_pass(3, 2, False, True)
    for k in order:
        t = wrap(tp + k)
        arrived(pre.at[t], prr.at[t])

    center = jnp.sum(pre[0].astype(F32), axis=1, keepdims=True)
    for t in range(1, N):
        center = center + jnp.sum(pre[t].astype(F32), axis=1, keepdims=True)
    center = center / D
    spread = jnp.zeros((ROWS, 1), F32)
    for t in range(N):
        shifted = pre[t].astype(F32) - center
        spread = spread + jnp.sum(shifted * shifted, axis=1, keepdims=True)
    scale = lax.rsqrt(spread / D + EPS_NORM)

    def normed_cols(t):
        return ((pre[t].astype(F32) - center) * scale * norm1_gain[:, t * COLS : (t + 1) * COLS]).astype(BF16)

    own = (pre[tp].astype(F32) - center) * scale * norm1_gain[:, of_tp(tp)]
    first_own[...] = own.astype(BF16)

    @pl.when(core == 0)
    def _():
        for t in range(N):
            first[HALO:, t * COLS : (t + 1) * COLS] = normed_cols(t)

    @pl.when(core == 1)
    def _():
        for t in range(N):
            value = normed_cols(t)
            for g in range(N):
                first[HALO:, g * COLS + t * 32 : g * COLS + (t + 1) * 32] = value[:, g * 32 : (g + 1) * 32]

    send(first.at[ROWS : ROWS + HALO], first.at[0:HALO], hls.at[0], hlr.at[0], nxt)
    wgt_pass(3, 1, True, False)
    wgt_pass(3, 3, False, True)
    arrived(first.at[0:HALO], hlr.at[0])

    def project(i):
        b = wrap(beta + offset(i))
        return dot(first[:, of_tp(b)], wgt[b].reshape(COLS, 2 * UNITS))

    def project_more(begin, end):
        def body(i, carry):
            up[...] += project(i)
            return carry

        lax.fori_loop(begin, end, body, 0)

    up[...] = jnp.zeros_like(up)
    project_more(0, 5)
    for b, p in (
        (wrap(beta + N - 3), 2),
        (wrap(beta + N - 3), 3),
        (wrap(beta + 3), 0),
        (wrap(beta + 3), 1),
    ):
        arrived(wgt_piece(b, p), w2r.at[4 * b + p])
    project_more(5, 7)
    b = wrap(beta + 4)
    for p in range(4):
        arrived(wgt_piece(b, p), w2r.at[4 * b + p])
    project_more(7, 8)

    up[...] = up[...].astype(BF16).astype(F32)

    @pl.when(sp == 0)
    def _():
        up[0:HALO, :] = jnp.zeros((HALO, 2 * UNITS), F32)

    def conv(taps, at, width):
        value = taps[0:1] * up[HALO - 2 : HALO - 2 + ROWS, at : at + width]
        value = value + taps[1:2] * up[HALO - 1 : HALO - 1 + ROWS, at : at + width]
        return value + taps[2:3] * up[HALO : HALO + ROWS, at : at + width]

    def gated(g, v):
        return (g / (1.0 + jnp.exp(-g)) * v).astype(BF16)

    for at in range(0, MAIN, 128):
        g = conv(conv_gate[:, at : at + 128], at, 128)
        v = conv(conv_val[:, at : at + 128], MAIN + at, 128)
        hidden[:, at : at + 128] = gated(g, v)
    taps = jnp.concatenate([conv_gate[:, MAIN:], conv_val[:, MAIN:]], axis=1)
    both = conv(taps, 2 * MAIN, 128)
    hidden[:, MAIN:] = gated(both[:, :64], both[:, 64:])

    local[2].wait()
    for k in order:
        t = wrap(tp + k)
        down_out[t] = dot(hidden[...], w_down[:, of_tp(t)]).astype(BF16)
        send(down_out.at[t], down_in.at[tp], dns.at[k], dnr.at[tp], along_tp(k))
    value = dot(hidden[...], w_down[:, of_tp(tp)]) + ALPHA * first_own[...].astype(F32)
    for k in order:
        t = wrap(tp + k)
        arrived(down_in.at[t], dnr.at[t])
        value = value + down_in[t].astype(F32)

    amount = jnp.sum(value, axis=1, keepdims=True)
    apart = value - amount / COLS
    apart = jnp.sum(apart * apart, axis=1, keepdims=True)
    line = lax.broadcasted_iota(jnp.int32, (8, ROWS), 0)
    stats[tp] = jnp.where(
        line == 0,
        jnp.broadcast_to(amount, (ROWS, ROWS)).T[0:8],
        jnp.broadcast_to(apart, (ROWS, ROWS)).T[0:8],
    )
    for k in order:
        send(stats.at[tp], stats.at[tp], sts.at[k], srr.at[tp], along_tp(k))
    for k in order:
        t = wrap(tp + k)
        arrived(stats.at[t], srr.at[t])
    whole = stats[0]
    for t in range(1, N):
        whole = whole + stats[t]
    center = whole[0:1] / D
    spread = whole[1:2]
    for t in range(N):
        gap = stats[t][0:1] / COLS - center
        spread = spread + COLS * gap * gap
    scale = lax.rsqrt(spread / D + EPS_NORM)
    center = jnp.broadcast_to(center, (ROWS, ROWS)).T[:, 0:1]
    scale = jnp.broadcast_to(scale, (ROWS, ROWS)).T[:, 0:1]
    out[...] = ((value - center) * scale * norm2_gain[...]).astype(BF16)

    for copy in pending:
        copy.wait_send()


def shards(*args):
    (
        resid,
        qa_nope,
        qb_nope,
        qa_rope,
        qb_rope,
        latent,
        key_rope,
        lat_gain,
        wa_key,
        wa_val,
        wb_key,
        wb_val,
        gain_a,
        gain_b,
        wa_out,
        wb_out,
        norm1_gain,
        ffn_gate,
        ffn_val,
        conv_gate,
        conv_val,
        ffn_down,
        norm2_gain,
    ) = args
    positions = lax.axis_index("sp") * ROWS + jnp.arange(ROWS)
    freq = THETA ** (-jnp.arange(DR // 2, dtype=F32) * 2.0 / DR)
    angle = positions.astype(F32)[:, None] * jnp.concatenate([freq, freq])[None, :]
    cosine = jnp.cos(angle)
    sign = jnp.where(jnp.arange(DR) < DR // 2, -1.0, 1.0).astype(F32)
    sine = jnp.sin(angle) * sign[None, :]
    vmem = pl.BlockSpec(memory_space=pltpu.VMEM)
    anywhere = pl.BlockSpec(memory_space=pl.ANY)
    operands = (
        cosine,
        sine,
        resid,
        qa_nope,
        qb_nope,
        qa_rope,
        qb_rope,
        latent,
        key_rope,
        lat_gain[None],
        wa_key,
        wa_val,
        wb_key,
        wb_val,
        gain_a[None],
        gain_b[None],
        wa_out,
        wb_out,
        norm1_gain[None],
        ffn_gate,
        ffn_val,
        conv_gate,
        conv_val,
        ffn_down,
        norm2_gain[None],
    )
    specs = [vmem] * len(operands)
    for at in (16, 17, 23):
        specs[at] = anywhere
    dma = pltpu.SemaphoreType.DMA
    return pl.pallas_call(
        kernel,
        out_shape=jax.ShapeDtypeStruct((ROWS, COLS), BF16),
        in_specs=specs,
        out_specs=vmem,
        scratch_shapes=[
            pltpu.VMEM((2, N, N, 144, 128), BF16),
            pltpu.VMEM((N, N, 32, 2 * UNITS), BF16),
            pltpu.VMEM((3 * ROWS, LAT), BF16),
            pltpu.VMEM((3 * ROWS, DR), BF16),
            pltpu.VMEM((3 * ROWS, LAT), F32),
            pltpu.VMEM((3 * ROWS, 128), F32),
            pltpu.VMEM((3 * ROWS, 128), F32),
            pltpu.VMEM((256, D), BF16),
            pltpu.VMEM((UNITS, D), BF16),
            pltpu.VMEM((N, ROWS, COLS), BF16),
            pltpu.VMEM((N, ROWS, COLS), BF16),
            pltpu.VMEM((N, 8, ROWS), F32),
            pltpu.VMEM((N, ROWS, COLS), BF16),
            pltpu.VMEM((HALO + ROWS, D), BF16),
            pltpu.VMEM((ROWS, COLS), BF16),
            pltpu.VMEM((HALO + ROWS, 2 * UNITS), F32),
            pltpu.VMEM((ROWS, UNITS), BF16),
            pltpu.VMEM((N, ROWS, COLS), BF16),
            pltpu.VMEM((N, ROWS, COLS), BF16),
            pltpu.VMEM((N, 8, ROWS), F32),
            dma((3,)),
            dma((7,)),
            dma((8,)),
            dma((8,)),
            dma((8,)),
            dma((14,)),
            dma((16,)),
            dma((8,)),
            dma((8,)),
            dma((28,)),
            dma((32,)),
            dma((8,)),
            dma((8,)),
            dma((8,)),
            dma((8,)),
            dma((8,)),
            dma((8,)),
            dma((1,)),
            dma((1,)),
            dma((8,)),
            dma((8,)),
            dma((8,)),
            dma((8,)),
        ],
        compiler_params=pltpu.CompilerParams(
            collective_id=0, has_side_effects=True, vmem_limit_bytes=56 * 1024 * 1024
        ),
        cost_estimate=pl.CostEstimate(flops=8_000_000_000, bytes_accessed=20_000_000, transcendentals=4_000_000),
    )(*operands)


def solution(mesh):
    return jax.shard_map(
        shards,
        mesh=mesh,
        in_specs=(
            P("sp", "tp"),
            P("sp", "tp"),
            P("sp", "tp"),
            P("sp", "tp"),
            P("sp", "tp"),
            P("sp", None),
            P("sp", None),
            P(),
            P(None, "tp"),
            P(None, "tp"),
            P(None, "tp"),
            P(None, "tp"),
            P("tp"),
            P("tp"),
            P("tp", None),
            P("tp", None),
            P(),
            P("sp", "tp"),
            P("sp", "tp"),
            P(None, "tp"),
            P(None, "tp"),
            P("tp", None),
            P("tp"),
        ),
        out_specs=P("sp", "tp"),
        check_vma=False,
    )
```

time: 242 us -> 105 us (0.43)
  blocking collectives: 113 us -> 0 us
  Pallas kernels: 0 us -> 98.2 us
  matrix products: 43.5 us -> 0 us
  waiting for transfers between devices: 40.9 us -> 0 us
  between operations: 13.8 us -> 0.01 us
  other arithmetic: 11.9 us -> 1.06 us
  starting transfers between devices: 10.4 us -> 0 us
    pallas_call x0 -> x1, Pallas kernels: none -> 98.2 us  [shards(): pl.pallas_call(kernel, out_shape=jax.ShapeDtypeStruct((ROWS, COLS), BF16)...]
    all_to_all x5 -> x0, blocking collectives: 65 us -> none  [the longest x3 34.5 us: from_everyone(): lax.all_to_all(jnp.broadcast_to(array[None], (count, *array.shape)), axis...]
    all_gather x1 -> x0, blocking collectives: 48.3 us -> none  [shards(): lax.all_gather(k_rot, 'sp', axis=0, tiled=True)]
    dot_general x13 -> x0, matrix products: 43.5 us -> none  [the longest x2 11.6 us: absorb(): jnp.einsum('hqk,khd->qhd', weights.astype(jnp.bfloat16), vals, preferred_...]
    all_gather x2 -> x0, waiting for transfers between devices: 34.5 us -> none  [the longest x1 31.7 us: shards(): lax.all_gather(lat_n, 'sp', axis=0, tiled=True)]
    ppermute x2 -> x0, starting transfers between devices: 6.16 us -> none  [passed_along(): lax.ppermute(value, axis, [(source, source + steps) for source in range(l...]
    all_to_all x1 -> x0, starting transfers between devices: 4.22 us -> none  [from_everyone(): lax.all_to_all(jnp.broadcast_to(array[None], (count, *array.shape)), axis...]
    all_to_all x1 -> x0, waiting for transfers between devices: 3.98 us -> none  [from_everyone(): lax.all_to_all(jnp.broadcast_to(array[None], (count, *array.shape)), axis...]
  transfers between devices with their start and end apart: 5 -> 0, of which waited for: 4 -> 0; matrix products, arithmetic and copies ran while one was open for 21% -> 0% of each run, Pallas kernels for 0% -> 0%
where the time goes in v1:
time: 105 us
  Pallas kernels  98.2 us (94%)
  local copies, waits for them, and re-layouts  5.71 us (5%)
  other arithmetic  1.06 us (1%)
    pallas_call x1, Pallas kernels, shards(): pl.pallas_call(kernel, out_shape=jax.ShapeDtypeStruct((ROWS, COLS), BF16)...  98.2 us
    unnamed x4, local copies, waits for them, and re-layouts  5.71 us

profile of v1, /device:TPU:1, one launch (start us, length us, event | category | flops | bytes accessed | tf_op | source)
XLA Modules:
  0.0 105.0 jit_solution(3385785456403313481)
XLA Ops:
  0.0 0.1 compare_select_fusion
  0.1 1.4 %copy.28.qa_rope = bf16[128,64]{1,0:T(8,128)(2,1)} copy(bf16[128,64]{0,1:T(8,128)(2,1)} %param.26) | data formatting | bytes 32768 | tf_op args[3]
  1.5 1.4 %copy.29.qb_rope = bf16[128,32]{1,0:T(8,128)(2,1)} copy(bf16[128,32]{0,1:T(8,128)(2,1)} %param.27) | data formatting | bytes 16384 | tf_op args[4]
  2.9 1.4 %copy.30.key_rope = bf16[128,32]{1,0:T(8,128)(2,1)} copy(bf16[128,32]{0,1:T(8,128)(2,1)} %param.29) | data formatting | bytes 16384 | tf_op args[6]
  4.3 1.0 fusion
  5.3 98.2 %shard_map.217 = bf16[128,256]{1,0:T(8,128)(2,1)} custom-call(f32[128,32]{1,0:T(8,128)} %get-tuple-element.6.cosine, f32[128,32]{1,0:T(8,128)} %get-tuple-element.5.sine, bf16[128,256]{1,0:T(8,128)(2,1)} %resid.1, bf16[128,128]{1,0:T(8,128)(2,1)} %qa_nope.1, bf16[128,128]{1,0:T(8,128)(2,1)} %qb_nope.1, bf16[128,64]{1,0:T(8,128)(2,1)} %copy.28.qa_rope, ...), custom_call_target="tpu_custom_call" | custom-call | flops 8000000000 | bytes 20000000 | tf_op jit(solution)/shard_map/pallas_call | solution.py:575
  103.5 1.5 %copy.32 = bf16[128,256]{1,0:T(8,128)(2,1)} copy(bf16[128,256]{1,0:T(8,128)(2,1)} %shard_map.217) | data formatting | bytes 131072
  (2 shorter events, 0.0 us)

commit v2 on v1

--- a/solution.py
+++ b/solution.py
@@ -1,5 +1,6 @@
 import jax
 import jax.numpy as jnp
+import numpy as np
 from jax import lax
 from jax.experimental import pallas as pl
 from jax.experimental.pallas import tpu as pltpu
@@ -39,13 +40,25 @@
     return lax.dot_general(a, b, (((1,), (1,)), ((), ())), preferred_element_type=F32)
 
 
+class Stages:
+    def __init__(self):
+        self.scope = None
+
+    def __call__(self, name):
+        if self.scope is not None:
+            self.scope.__exit__(None, None, None)
+        self.scope = None
+        if name:
+            self.scope = jax.named_scope(name)
+            self.scope.__enter__()
+
+
 def wrap(v):
     return lax.rem(v, N)
 
 
 def kernel(
-    cosine,
-    sine,
+    freq,
     resid,
     qa_nope,
     qb_nope,
@@ -83,6 +96,7 @@
     mix_in,
     energy,
     pre,
+    pre_halo,
     first,
     first_own,
     up,
@@ -99,6 +113,10 @@
     l2r,
     dds,
     ddr,
+    xss,
+    xsr,
+    xds,
+    xdr,
     w2s,
     w2r,
     mxs,
@@ -114,6 +132,8 @@
     sts,
     srr,
 ):
+    stage = Stages()
+    stage("enter")
     sp = lax.axis_index("sp")
     tp = lax.axis_index("tp")
     core = lax.rem(tp, 2)
@@ -124,6 +144,9 @@
     sa = 1 + 7 * core
     sb = 8 - 7 * core
     partner = (sp, tp + 1 - 2 * core)
+    sideways = (sp, wrap(tp + 2 + 4 * core))
+    parity = lax.rem(lax.div(tp, 2), 2)
+    part_of = 2 * parity + core
     nxt = (lax.rem(sp + 1, N * N), tp)
     prv = (lax.rem(sp + N * N - 1, N * N), tp)
 
@@ -153,7 +176,8 @@
 
     barrier = pltpu.get_barrier_semaphore()
     peers = [along_a(k) for k in range(1, N)] + [along_b(1), along_b(N - 1)]
-    peers += [along_tp(k) for k in range(1, N)] + [nxt, prv]
+    peers += [along_tp(k) for k in range(1, N)]
+    peers += [(line[0], t) for line in (nxt, prv) for t in range(N)]
     for device in peers:
         pl.semaphore_signal(barrier, inc=1, device_id=device, device_id_type=MESH)
 
@@ -165,30 +189,40 @@
     for copy in local:
         copy.start()
 
-    half = pl.ds(pl.multiple_of(core * 64, 64), 64)
-    wide = latent[half, :].astype(F32)
+    stage("prep")
+    quarter = pl.ds(pl.multiple_of(part_of * 32, 32), 32)
+    wide = latent[quarter, :].astype(F32)
     wide = wide * lax.rsqrt(jnp.mean(wide * wide, axis=1, keepdims=True) + EPS_RMS) * lat_gain[...]
     lat_n = wide.astype(BF16)
 
-    def rotated(v, c, s):
-        return v * c + jnp.concatenate([v[:, DR // 2 :], v[:, : DR // 2]], axis=1) * s
-
-    k_rot = rotated(key_rope[half, :].astype(F32), cosine[half, :], sine[half, :])
-    k_wide = jnp.concatenate([k_rot, jnp.zeros((64, 128 - DR), F32)], axis=1)
-    k_wide = jnp.concatenate([k_wide, jnp.zeros((64, 128), F32)], axis=0)
-    k_t = k_wide.T
-    k_packed = jnp.concatenate([k_t[0:16, 0:64], k_t[16:32, 0:64]], axis=1)
-    lat[core, beta, alpha, 0:64, :] = lat_n[:, :128]
-    lat[core, beta, alpha, 64:128, :] = lat_n[:, 128:]
-    lat[core, beta, alpha, 128:144, :] = k_packed.astype(BF16)
+    spots = sp * ROWS + lax.broadcasted_iota(jnp.int32, (DR // 2, ROWS), 1)
+    angle = spots.astype(F32) * freq[...]
+    cosine = jnp.cos(angle)
+    sine = jnp.sin(angle)
+
+    def rotated(v):
+        a = v[: DR // 2].astype(F32)
+        b = v[DR // 2 :].astype(F32)
+        return jnp.concatenate([a * cosine - b * sine, b * cosine + a * sine], axis=0)
+
+    k_t = rotated(key_rope[...])
+    k_packed = jnp.zeros((8, 128), F32)
+    for q in range(4):
+        taken = [k_t[8 * g : 8 * g + 8, 32 * q : 32 * q + 32] for g in range(4)]
+        k_packed = jnp.where(part_of == q, jnp.concatenate(taken, axis=1), k_packed)
+    lat[core, beta, alpha, 0:32, :] = lat_n[:, :128]
+    lat[core, beta, alpha, 32:64, :] = lat_n[:, 128:]
+    lat[core, beta, alpha, 64:80, :] = jnp.concatenate([k_packed, k_packed], axis=0).astype(BF16)
     wgt[beta, alpha, :, 0:MAIN] = ffn_gate[:, :MAIN]
     wgt[beta, alpha, :, MAIN : 2 * MAIN] = ffn_val[:, :MAIN]
     wgt[beta, alpha, :, 2 * MAIN :] = jnp.concatenate(
         [ffn_gate[:, MAIN:].astype(F32), ffn_val[:, MAIN:].astype(F32)], axis=1
     ).astype(BF16)
 
+    stage("barrier")
     pl.semaphore_wait(barrier, len(peers))
 
+    stage("send1")
     mine = lat.at[core, beta, alpha]
     for k in (4, 3, 5, 2, 6, 1, 7):
         send(mine, mine, l1s.at[k - 1], l1r.at[alpha], along_a(k))
@@ -207,20 +241,26 @@
 
     weight_step(0, True, True)
 
+    stage("queries")
     q_scale_a = (DA + DR) ** (-0.5) * LOG2E
     q_scale_b = (DB + DR) ** (-0.5) * LOG2E
     for h in range(2):
         part = dot_t(qa_nope[:, h * DA : (h + 1) * DA], wa_key[:, h * DA : (h + 1) * DA])
         q_lat[h * ROWS : (h + 1) * ROWS, :] = (part * q_scale_a).astype(BF16)
-        turned = rotated(qa_rope[:, h * DR : (h + 1) * DR].astype(F32), cosine[...], sine[...])
-        q_rot[h * ROWS : (h + 1) * ROWS, :] = (turned * q_scale_a).astype(BF16)
     part = dot_t(qb_nope[...], wb_key[...])
     q_lat[2 * ROWS :, :] = (part * q_scale_b).astype(BF16)
-    turned = rotated(qb_rope[...].astype(F32), cosine[...], sine[...])
-    q_rot[2 * ROWS :, :] = (turned * q_scale_b).astype(BF16)
+    turned = [rotated(qa_rope[h * DR : (h + 1) * DR]) * q_scale_a for h in range(2)]
+    turned += [rotated(qb_rope[...]) * q_scale_b, jnp.zeros((DR, ROWS), F32)]
+    turned = jnp.concatenate(turned, axis=0).T.astype(BF16)
+    for h in range(3):
+        q_rot[h * ROWS : (h + 1) * ROWS, :] = turned[:, h * DR : (h + 1) * DR]
     acc[...] = jnp.zeros_like(acc)
     top[...] = jnp.full_like(top, LOW)
     total[...] = jnp.zeros_like(total)
+
+    def offset(i):
+        steps = lax.div(i + 1, 2)
+        return wrap(N + steps * (1 - 2 * lax.rem(i, 2)))
 
     def lat_piece(b, p):
         return lat.at[core, b, pl.ds(4 * p, 4)]
@@ -237,7 +277,14 @@
                 send(lat_piece(b, p), lat_piece(b, p), l2s.at[at], l2r.at[2 * b + p], along_b(k))
 
     def hand_over(b):
+        send(lat.at[core, b], lat.at[3 - core, b], xss.at[b], xsr.at[b], sideways)
         send(lat.at[core, b], lat.at[core, b], dds.at[b], ddr.at[b], partner)
+
+    def pass_over(i):
+        b = wrap(beta + offset(i))
+        block = lat.at[3 - core, b]
+        arrived(block, xsr.at[b])
+        send(block, block, xds.at[b], xdr.at[b], partner)
 
     def wgt_piece(b, p):
         return wgt.at[b, pl.ds(2 * p, 2)]
@@ -253,71 +300,35 @@
                 at = base + 4 * d + (p if d < 3 or k == 1 else p - 2)
                 send(wgt_piece(b, p), wgt_piece(b, p), w2s.at[at], w2r.at[4 * b + p], along_b(k))
 
-    for k in range(1, N):
-        block = lat.at[core, beta, wrap(alpha + k)]
-        arrived(block, l1r.at[wrap(alpha + k)])
-    lat_pass(0, 0, True, True)
-    lat_pass(0, 1, True, True)
-    hand_over(beta)
-    weight_step(1, True, True)
-    weight_step(2, True, True)
-    lat_pass(1, 0, True, True)
-    weight_step(3, True, False)
-    lat_pass(1, 1, True, True)
-    hand_over(wrap(beta + N - 1))
-    hand_over(wrap(beta + 1))
-    lat_pass(2, 0, True, True)
-    for k in (3, 4):
-        a = wrap(alpha + k)
-        arrived(wgt.at[beta, a], w1r.at[a])
-    wgt_pass(0, 0)
-    lat_pass(2, 1, True, True)
-    hand_over(wrap(beta + N - 2))
-    hand_over(wrap(beta + 2))
-    wgt_pass(0, 1)
-    lat_pass(3, 0, True, False)
-    lat_pass(3, 1, False, True)
-    wgt_pass(0, 2)
-    wgt_pass(0, 3)
-    for b, p in ((wrap(beta + N - 3), 1), (wrap(beta + 3), 0)):
-        arrived(lat_piece(b, p), l2r.at[2 * b + p])
-    hand_over(wrap(beta + N - 3))
-    hand_over(wrap(beta + 3))
-    b = wrap(beta + 4)
-    arrived(lat_piece(b, 0), l2r.at[2 * b])
-    arrived(lat_piece(b, 1), l2r.at[2 * b + 1])
-    hand_over(b)
-
-    def offset(i):
-        steps = lax.div(i + 1, 2)
-        return wrap(N + steps * (1 - 2 * lax.rem(i, 2)))
-
     def attend(i):
         b0 = wrap(z + offset(i))
         b1 = wrap(y + offset(i))
-        theirs = b1 + core * (b0 - b1)
+        theirs = wrap(alpha + offset(i))
         arrived(lat.at[1 - core, theirs], ddr.at[theirs])
+        arrived(lat.at[2 + core, theirs], xdr.at[theirs])
         left, right, roped = [], [], []
-        for half_of, b in ((0, b0), (1, b1)):
-            left.append(lat[half_of, b, :, 0:64, :].reshape(512, 128))
-            right.append(lat[half_of, b, :, 64:128, :].reshape(512, 128))
-            x = lat[half_of, b, :, 128:144, :]
-            upper = [jnp.concatenate([x[a][:, :64], x[a + 1][:, :64]], axis=1) for a in range(0, N, 2)]
-            lower = [jnp.concatenate([x[a][:, 64:], x[a + 1][:, 64:]], axis=1) for a in range(0, N, 2)]
-            roped.append(
-                jnp.concatenate(
-                    [jnp.concatenate(upper, axis=1), jnp.concatenate(lower, axis=1)], axis=0
-                )
-            )
+        for slot, b in ((0, b0), (1, b1), (2, b1), (3, b0)):
+            left.append(lat[slot, b, :, 0:32, :].reshape(256, 128))
+            right.append(lat[slot, b, :, 32:64, :].reshape(256, 128))
+            x = lat[slot, b, :, 64:80, :].astype(F32)
+            for quad in range(0, N, 4):
+                lines = [
+                    jnp.concatenate([x[a][0:8, 32 * g : 32 * g + 32] for a in range(quad, quad + 4)], axis=1)
+                    for g in range(4)
+                ]
+                roped.append(jnp.concatenate(lines, axis=0).astype(BF16))
         keys = jnp.concatenate(
             [jnp.concatenate(left, axis=0), jnp.concatenate(right, axis=0)], axis=1
         )
         ropes = jnp.concatenate(roped, axis=1)
         scores = dot_t(q_lat[...], keys) + dot(q_rot[...], ropes)
         j = lax.broadcasted_iota(jnp.int32, (1, 1024), 1)
-        a = lax.shift_right_logical(lax.bitwise_and(j, 511), 6)
-        r = lax.bitwise_and(j, 63)
-        spots = jnp.where(j < 512, b0 * 1024 + a * 128 + r, a * 1024 + b1 * 128 + 64 + r)
+        slot = lax.shift_right_logical(j, 8)
+        a = lax.bitwise_and(lax.shift_right_logical(j, 5), 7)
+        r = lax.bitwise_and(j, 31)
+        block = jnp.where((slot == 0) | (slot == 3), b0 * N + a, a * N + b1)
+        which = jnp.where(slot < 2, 2 * parity + slot, 5 - 2 * parity - slot)
+        spots = block * ROWS + which * 32 + r
         rows = lax.broadcasted_iota(jnp.int32, (3 * ROWS, 1), 0)
         rows = sp * ROWS + lax.bitwise_and(rows, ROWS - 1)
         scores = jnp.where(spots <= rows, scores, LOW)
@@ -329,17 +340,96 @@
         acc[...] = acc[...] * shrink + dot(weights.astype(BF16), keys)
         top[...] = jnp.broadcast_to(new, top.shape)
 
-    def attend_two(e):
-        def body(i, carry):
-            attend(i)
-            return carry
-
-        lax.fori_loop(2 * e, 2 * e + 2, body, 0)
-
-    for e in range(4):
-        attend_two(e)
-        wgt_pass(1, e)
-
+    stage("lat1")
+    for k in range(1, N):
+        block = lat.at[core, beta, wrap(alpha + k)]
+        arrived(block, l1r.at[wrap(alpha + k)])
+    stage("ring0")
+    lat_pass(0, 0, True, True)
+    lat_pass(0, 1, True, True)
+    hand_over(beta)
+    stage("w1_1")
+    weight_step(1, True, True)
+    stage("ring1a")
+    lat_pass(1, 0, True, True)
+    stage("ring1b")
+    lat_pass(1, 1, True, True)
+    hand_over(wrap(beta + N - 1))
+    hand_over(wrap(beta + 1))
+    stage("over0")
+    pass_over(0)
+    stage("w1_2")
+    weight_step(2, True, True)
+    stage("attend0")
+    attend(0)
+    stage("ring2a")
+    lat_pass(2, 0, True, True)
+    stage("ring2b")
+    lat_pass(2, 1, True, True)
+    hand_over(wrap(beta + N - 2))
+    hand_over(wrap(beta + 2))
+    stage("w1_3")
+    weight_step(3, True, False)
+    stage("over1")
+    pass_over(1)
+    stage("over2")
+    pass_over(2)
+    stage("attend1")
+    attend(1)
+    stage("ring3")
+    lat_pass(3, 0, True, False)
+    lat_pass(3, 1, False, True)
+    stage("w1_4")
+    for k in (3, 4):
+        a = wrap(alpha + k)
+        arrived(wgt.at[beta, a], w1r.at[a])
+    wgt_pass(0, 0)
+    wgt_pass(0, 1)
+    stage("attend2")
+    attend(2)
+    stage("ring3end")
+    for b, p in ((wrap(beta + N - 3), 1), (wrap(beta + 3), 0)):
+        arrived(lat_piece(b, p), l2r.at[2 * b + p])
+    hand_over(wrap(beta + N - 3))
+    hand_over(wrap(beta + 3))
+    stage("over3")
+    pass_over(3)
+    wgt_pass(0, 2)
+    stage("ring4")
+    b = wrap(beta + 4)
+    arrived(lat_piece(b, 0), l2r.at[2 * b])
+    arrived(lat_piece(b, 1), l2r.at[2 * b + 1])
+    hand_over(b)
+    wgt_pass(0, 3)
+    stage("over4")
+    pass_over(4)
+    stage("attend3")
+    attend(3)
+    stage("pass1_0")
+    wgt_pass(1, 0)
+    stage("over5")
+    pass_over(5)
+    stage("attend4")
+    attend(4)
+    stage("pass1_1")
+    wgt_pass(1, 1)
+    stage("over6")
+    pass_over(6)
+    stage("attend5")
+    attend(5)
+    stage("pass1_2")
+    wgt_pass(1, 2)
+    stage("over7")
+    pass_over(7)
+    stage("attend6")
+    attend(6)
+    stage("pass1_3")
+    wgt_pass(1, 3)
+    stage("attend7")
+    attend(7)
+    stage("pass2_0")
+    wgt_pass(2, 0)
+    stage("heads")
     normed = (acc[...] / total[:, 0:1]).astype(BF16)
     raw_a = jnp.concatenate(
         [dot(normed[h * ROWS : (h + 1) * ROWS], wa_val[:, h * DA : (h + 1) * DA]) for h in range(2)], axis=1
@@ -354,6 +444,7 @@
     def of_tp(t):
         return pl.ds(pl.multiple_of(t * COLS, COLS), COLS)
 
+    stage("mixsend")
     order = (4, 5, 3, 2, 6, 7, 1)
     for k in order:
         t = wrap(tp + k)
@@ -361,41 +452,65 @@
         send(mix_out.at[t], mix_in.at[tp], mxs.at[k], mxr.at[tp], along_tp(k))
         send(energy.at[tp], energy.at[tp], ens.at[k], enr.at[tp], along_tp(k))
     mix = dot(gained, w_out[:, of_tp(tp)])
-    wgt_pass(2, 0)
+    stage("pass2_123")
     wgt_pass(2, 1)
+    wgt_pass(2, 2)
+    wgt_pass(2, 3)
+    stage("mixwait")
     for k in order:
         t = wrap(tp + k)
         arrived(mix_in.at[t], mxr.at[t])
         arrived(energy.at[t], enr.at[t])
         mix = mix + mix_in[t].astype(F32)
+    stage("mixsum")
     power = energy[0]
     for t in range(1, N):
         power = power + energy[t]
     factor = lax.rsqrt(power[0:1] / (HA * DA + HB * DB) + EPS_RMS)
     factor = jnp.broadcast_to(factor, (ROWS, ROWS)).T[:, 0:1]
     pre[tp] = (ALPHA * resid[...].astype(F32) + mix * factor).astype(BF16)
-    for k in order:
+    for k in (4, 2, 6):
         send(pre.at[tp], pre.at[tp], prs.at[k], prr.at[tp], along_tp(k))
-    wgt_pass(2, 2)
-    wgt_pass(2, 3)
+    send(pre.at[tp], pre.at[tp], prs.at[1], prr.at[tp], partner)
+    for t in range(N):
+        send(pre.at[tp, ROWS - HALO : ROWS], pre_halo.at[tp], hls.at[t], hlr.at[tp], (nxt[0], t))
+    stage("pass3")
     wgt_pass(3, 0, True, False)
     wgt_pass(3, 2, False, True)
-    for k in order:
+    wgt_pass(3, 1, True, False)
+    wgt_pass(3, 3, False, True)
+    stage("prewait")
+    for k in (2, 6, 4):
         t = wrap(tp + k)
         arrived(pre.at[t], prr.at[t])
-
-    center = jnp.sum(pre[0].astype(F32), axis=1, keepdims=True)
-    for t in range(1, N):
-        center = center + jnp.sum(pre[t].astype(F32), axis=1, keepdims=True)
-    center = center / D
-    spread = jnp.zeros((ROWS, 1), F32)
+        send(pre.at[t], pre.at[t], prs.at[k + 1], prr.at[t], partner)
+    stage("halowait")
     for t in range(N):
-        shifted = pre[t].astype(F32) - center
-        spread = spread + jnp.sum(shifted * shifted, axis=1, keepdims=True)
-    scale = lax.rsqrt(spread / D + EPS_NORM)
+        arrived(pre_halo.at[t], hlr.at[t])
+    stage("prewait2")
+    for k in (1, 3, 5, 7):
+        t = wrap(tp + k)
+        arrived(pre.at[t], prr.at[t])
+
+    stage("norm1")
+    def row_stats(ref):
+        middle = jnp.sum(ref[0].astype(F32), axis=1, keepdims=True)
+        for t in range(1, N):
+            middle = middle + jnp.sum(ref[t].astype(F32), axis=1, keepdims=True)
+        middle = middle / D
+        wide = jnp.zeros_like(middle)
+        for t in range(N):
+            shifted = ref[t].astype(F32) - middle
+            wide = wide + jnp.sum(shifted * shifted, axis=1, keepdims=True)
+        return middle, lax.rsqrt(wide / D + EPS_NORM)
+
+    center, scale = row_stats(pre)
+    center_halo, scale_halo = row_stats(pre_halo)
 
     def normed_cols(t):
-        return ((pre[t].astype(F32) - center) * scale * norm1_gain[:, t * COLS : (t + 1) * COLS]).astype(BF16)
+        gain = norm1_gain[:, t * COLS : (t + 1) * COLS]
+        above = (pre_halo[t].astype(F32) - center_halo) * scale_halo * gain
+        return jnp.concatenate([above, (pre[t].astype(F32) - center) * scale * gain], axis=0).astype(BF16)
 
     own = (pre[tp].astype(F32) - center) * scale * norm1_gain[:, of_tp(tp)]
     first_own[...] = own.astype(BF16)
@@ -403,19 +518,14 @@
     @pl.when(core == 0)
     def _():
         for t in range(N):
-            first[HALO:, t * COLS : (t + 1) * COLS] = normed_cols(t)
+            first[:, t * COLS : (t + 1) * COLS] = normed_cols(t)
 
     @pl.when(core == 1)
     def _():
         for t in range(N):
             value = normed_cols(t)
             for g in range(N):
-                first[HALO:, g * COLS + t * 32 : g * COLS + (t + 1) * 32] = value[:, g * 32 : (g + 1) * 32]
-
-    send(first.at[ROWS : ROWS + HALO], first.at[0:HALO], hls.at[0], hlr.at[0], nxt)
-    wgt_pass(3, 1, True, False)
-    wgt_pass(3, 3, False, True)
-    arrived(first.at[0:HALO], hlr.at[0])
+                first[:, g * COLS + t * 32 : g * COLS + (t + 1) * 32] = value[:, g * 32 : (g + 1) * 32]
 
     def project(i):
         b = wrap(beta + offset(i))
@@ -428,8 +538,10 @@
 
         lax.fori_loop(begin, end, body, 0)
 
+    stage("up5")
     up[...] = jnp.zeros_like(up)
     project_more(0, 5)
+    stage("wait3")
     for b, p in (
         (wrap(beta + N - 3), 2),
         (wrap(beta + N - 3), 3),
@@ -437,12 +549,16 @@
         (wrap(beta + 3), 1),
     ):
         arrived(wgt_piece(b, p), w2r.at[4 * b + p])
+    stage("up7")
     project_more(5, 7)
+    stage("wait4")
     b = wrap(beta + 4)
     for p in range(4):
         arrived(wgt_piece(b, p), w2r.at[4 * b + p])
+    stage("up8")
     project_more(7, 8)
 
+    stage("conv")
     up[...] = up[...].astype(BF16).astype(F32)
 
     @pl.when(sp == 0)
@@ -465,17 +581,20 @@
     both = conv(taps, 2 * MAIN, 128)
     hidden[:, MAIN:] = gated(both[:, :64], both[:, 64:])
 
+    stage("down")
     local[2].wait()
     for k in order:
         t = wrap(tp + k)
         down_out[t] = dot(hidden[...], w_down[:, of_tp(t)]).astype(BF16)
         send(down_out.at[t], down_in.at[tp], dns.at[k], dnr.at[tp], along_tp(k))
     value = dot(hidden[...], w_down[:, of_tp(tp)]) + ALPHA * first_own[...].astype(F32)
+    stage("downwait")
     for k in order:
         t = wrap(tp + k)
         arrived(down_in.at[t], dnr.at[t])
         value = value + down_in[t].astype(F32)
 
+    stage("stats")
     amount = jnp.sum(value, axis=1, keepdims=True)
     apart = value - amount / COLS
     apart = jnp.sum(apart * apart, axis=1, keepdims=True)
@@ -487,9 +606,11 @@
     )
     for k in order:
         send(stats.at[tp], stats.at[tp], sts.at[k], srr.at[tp], along_tp(k))
+    stage("statswait")
     for k in order:
         t = wrap(tp + k)
         arrived(stats.at[t], srr.at[t])
+    stage("finish")
     whole = stats[0]
     for t in range(1, N):
         whole = whole + stats[t]
@@ -503,8 +624,10 @@
     scale = jnp.broadcast_to(scale, (ROWS, ROWS)).T[:, 0:1]
     out[...] = ((value - center) * scale * norm2_gain[...]).astype(BF16)
 
+    stage("drain")
     for copy in pending:
         copy.wait_send()
+    stage(None)
 
 
 def shards(*args):
@@ -533,24 +656,19 @@
         ffn_down,
         norm2_gain,
     ) = args
-    positions = lax.axis_index("sp") * ROWS + jnp.arange(ROWS)
-    freq = THETA ** (-jnp.arange(DR // 2, dtype=F32) * 2.0 / DR)
-    angle = positions.astype(F32)[:, None] * jnp.concatenate([freq, freq])[None, :]
-    cosine = jnp.cos(angle)
-    sign = jnp.where(jnp.arange(DR) < DR // 2, -1.0, 1.0).astype(F32)
-    sine = jnp.sin(angle) * sign[None, :]
+    freq = np.float64(THETA) ** (-np.arange(DR // 2) * 2.0 / DR)
+    freq = jnp.asarray(np.broadcast_to(freq[:, None], (DR // 2, ROWS)).astype(np.float32))
     vmem = pl.BlockSpec(memory_space=pltpu.VMEM)
     anywhere = pl.BlockSpec(memory_space=pl.ANY)
     operands = (
-        cosine,
-        sine,
+        freq,
         resid,
         qa_nope,
         qb_nope,
-        qa_rope,
-        qb_rope,
+        qa_rope.T,
+        qb_rope.T,
         latent,
-        key_rope,
+        key_rope.T,
         lat_gain[None],
         wa_key,
         wa_val,
@@ -569,7 +687,7 @@
         norm2_gain[None],
     )
     specs = [vmem] * len(operands)
-    for at in (16, 17, 23):
+    for at in (15, 16, 22):
         specs[at] = anywhere
     dma = pltpu.SemaphoreType.DMA
     return pl.pallas_call(
@@ -578,7 +696,7 @@
         in_specs=specs,
         out_specs=vmem,
         scratch_shapes=[
-            pltpu.VMEM((2, N, N, 144, 128), BF16),
+            pltpu.VMEM((4, N, N, 80, 128), BF16),
             pltpu.VMEM((N, N, 32, 2 * UNITS), BF16),
             pltpu.VMEM((3 * ROWS, LAT), BF16),
             pltpu.VMEM((3 * ROWS, DR), BF16),
@@ -591,6 +709,7 @@
             pltpu.VMEM((N, ROWS, COLS), BF16),
             pltpu.VMEM((N, 8, ROWS), F32),
             pltpu.VMEM((N, ROWS, COLS), BF16),
+            pltpu.VMEM((N, HALO, COLS), BF16),
             pltpu.VMEM((HALO + ROWS, D), BF16),
             pltpu.VMEM((ROWS, COLS), BF16),
             pltpu.VMEM((HALO + ROWS, 2 * UNITS), F32),
@@ -607,6 +726,10 @@
             dma((16,)),
             dma((8,)),
             dma((8,)),
+            dma((8,)),
+            dma((8,)),
+            dma((8,)),
+            dma((8,)),
             dma((28,)),
             dma((32,)),
             dma((8,)),
@@ -615,8 +738,8 @@
             dma((8,)),
             dma((8,)),
             dma((8,)),
-            dma((1,)),
-            dma((1,)),
+            dma((8,)),
+            dma((8,)),
             dma((8,)),
             dma((8,)),
             dma((8,)),

time: 105 us -> 86.1 us (0.82)
  Pallas kernels: 98.2 us -> 84.4 us
  local copies, waits for them, and re-layouts: 5.71 us -> 1.47 us
  other arithmetic: 1.06 us -> 0 us
    pallas_call x1, Pallas kernels: 98.2 us -> 84.4 us  [shards(): pl.pallas_call(kernel, out_shape=jax.ShapeDtypeStruct((ROWS, COLS), BF16)...]
    unnamed x4 -> x1, local copies, waits for them, and re-layouts: 5.71 us -> 1.47 us
where the time goes in v2:
time: 86.1 us; the launch traced here: 85.9 us
  Pallas kernels  84.4 us (98%)
  local copies, waits for them, and re-layouts  1.47 us (2%)
    pallas_call x1, Pallas kernels, shards(): pl.pallas_call(kernel, out_shape=jax.ShapeDtypeStruct((ROWS, COLS), BF16)...  84.4 us

profile of v2, /device:TPU:1, one launch (start us, length us, event | category | flops | bytes accessed | tf_op | source)
XLA Modules:
  0.0 85.9 jit_solution(5762880980292794102)
XLA Ops:
  0.0 84.4 %shard_map.226 = bf16[128,256]{1,0:T(8,128)(2,1)} custom-call(f32[16,128]{1,0:T(8,128)} %constant.2.clone.freq, bf16[128,256]{1,0:T(8,128)(2,1)} %resid.1, bf16[128,128]{1,0:T(8,128)(2,1)} %qa_nope.1, bf16[128,128]{1,0:T(8,128)(2,1)} %qb_nope.1, bf16[64,128]{1,0:T(8,128)(2,1)} %bitcast.8, bf16[32,128]{1,0:T(8,128)(2,1)} %bitcast.9, bf16[128,256]{1,0:T(8,128)(2,1)} %latent.1, ...), custom_call_target="tpu_custom_call" | custom-call | flops 8000000000 | bytes 20000000 | tf_op jit(solution)/shard_map/pallas_call | solution.py:693
  84.4 1.5 %copy.26 = bf16[128,256]{1,0:T(8,128)(2,1)} copy(bf16[128,256]{1,0:T(8,128)(2,1)} %shard_map.226) | data formatting | bytes 131072

commit v3 on v2

--- a/solution.py
+++ b/solution.py
@@ -58,30 +58,30 @@
 
 
 def kernel(
-    freq,
-    resid,
-    qa_nope,
-    qb_nope,
-    qa_rope,
-    qb_rope,
-    latent,
-    key_rope,
-    lat_gain,
-    wa_key,
-    wa_val,
-    wb_key,
-    wb_val,
-    gain_a,
-    gain_b,
+    freq_hbm,
+    resid_hbm,
+    qa_nope_hbm,
+    qb_nope_hbm,
+    qa_rope_hbm,
+    qb_rope_hbm,
+    latent_hbm,
+    key_rope_hbm,
+    lat_gain_hbm,
+    wa_key_hbm,
+    wa_val_hbm,
+    wb_key_hbm,
+    wb_val_hbm,
+    gain_a_hbm,
+    gain_b_hbm,
     wa_out,
     wb_out,
-    norm1_gain,
-    ffn_gate,
-    ffn_val,
-    conv_gate,
-    conv_val,
+    norm1_gain_hbm,
+    ffn_gate_hbm,
+    ffn_val_hbm,
+    conv_gate_hbm,
+    conv_val_hbm,
     ffn_down,
-    norm2_gain,
+    norm2_gain_hbm,
     out,
     lat,
     wgt,
@@ -93,6 +93,7 @@
     w_out,
     w_down,
     mix_out,
+    mix_pair,
     mix_in,
     energy,
     pre,
@@ -102,6 +103,7 @@
     up,
     hidden,
     down_out,
+    down_pair,
     down_in,
     stats,
     local_sem,
@@ -131,6 +133,32 @@
     dnr,
     sts,
     srr,
+    mps,
+    mpr,
+    dps,
+    dpr,
+    input_sem,
+    freq,
+    resid,
+    qa_nope,
+    qb_nope,
+    qa_rope,
+    qb_rope,
+    latent,
+    key_rope,
+    lat_gain,
+    wa_key,
+    wa_val,
+    wb_key,
+    wb_val,
+    gain_a,
+    gain_b,
+    norm1_gain,
+    ffn_gate,
+    ffn_val,
+    conv_gate,
+    conv_val,
+    norm2_gain,
 ):
     stage = Stages()
     stage("enter")
@@ -186,8 +214,34 @@
         pltpu.make_async_copy(wb_out, w_out.at[128:256], local_sem.at[1]),
         pltpu.make_async_copy(ffn_down, w_down, local_sem.at[2]),
     ]
-    for copy in local:
+    given = [
+        (freq_hbm, freq),
+        (resid_hbm, resid),
+        (qa_nope_hbm, qa_nope),
+        (qb_nope_hbm, qb_nope),
+        (qa_rope_hbm, qa_rope),
+        (qb_rope_hbm, qb_rope),
+        (latent_hbm, latent),
+        (key_rope_hbm, key_rope),
+        (lat_gain_hbm, lat_gain),
+        (wa_key_hbm, wa_key),
+        (wa_val_hbm, wa_val),
+        (wb_key_hbm, wb_key),
+        (wb_val_hbm, wb_val),
+        (gain_a_hbm, gain_a),
+        (gain_b_hbm, gain_b),
+        (norm1_gain_hbm, norm1_gain),
+        (ffn_gate_hbm, ffn_gate),
+        (ffn_val_hbm, ffn_val),
+        (conv_gate_hbm, conv_gate),
+        (conv_val_hbm, conv_val),
+        (norm2_gain_hbm, norm2_gain),
+    ]
+    entering = [pltpu.make_async_copy(src, dst, input_sem.at[at]) for at, (src, dst) in enumerate(given)]
+    for copy in entering + local:
         copy.start()
+    for copy in entering:
+        copy.wait()
 
     stage("prep")
     quarter = pl.ds(pl.multiple_of(part_of * 32, 32), 32)
@@ -287,7 +341,8 @@
         send(block, block, xds.at[b], xdr.at[b], partner)
 
     def wgt_piece(b, p):
-        return wgt.at[b, pl.ds(2 * p, 2)]
+        pair = lax.rem(lax.div(alpha, 2) + (0, 3, 1, 2)[p], 4)
+        return wgt.at[b, pl.ds(2 * pair, 2)]
 
     def wgt_pass(d, p, forward=True, backward=True):
         for go, b, k, base in (
@@ -300,44 +355,51 @@
                 at = base + 4 * d + (p if d < 3 or k == 1 else p - 2)
                 send(wgt_piece(b, p), wgt_piece(b, p), w2s.at[at], w2r.at[4 * b + p], along_b(k))
 
-    def attend(i):
-        b0 = wrap(z + offset(i))
-        b1 = wrap(y + offset(i))
-        theirs = wrap(alpha + offset(i))
-        arrived(lat.at[1 - core, theirs], ddr.at[theirs])
-        arrived(lat.at[2 + core, theirs], xdr.at[theirs])
-        left, right, roped = [], [], []
-        for slot, b in ((0, b0), (1, b1), (2, b1), (3, b0)):
-            left.append(lat[slot, b, :, 0:32, :].reshape(256, 128))
-            right.append(lat[slot, b, :, 32:64, :].reshape(256, 128))
+    def attend(*steps):
+        stage(f"attend{steps[-1]}")
+        places = []
+        for i in steps:
+            b0 = wrap(z + offset(i))
+            b1 = wrap(y + offset(i))
+            theirs = wrap(alpha + offset(i))
+            arrived(lat.at[1 - core, theirs], ddr.at[theirs])
+            arrived(lat.at[2 + core, theirs], xdr.at[theirs])
+            places += [(0, b0), (1, b1), (2, b1), (3, b0)]
+        rows = lax.broadcasted_iota(jnp.int32, (3 * ROWS, 1), 0)
+        rows = sp * ROWS + lax.bitwise_and(rows, ROWS - 1)
+        j = lax.broadcasted_iota(jnp.int32, (1, 256), 1)
+        a = lax.shift_right_logical(j, 5)
+        r = lax.bitwise_and(j, 31)
+        old = top[:, 0:1]
+        new = old
+        keys, scores = [], []
+        for slot, b in places:
+            left = lat[slot, b, :, 0:32, :].reshape(256, 128)
+            right = lat[slot, b, :, 32:64, :].reshape(256, 128)
+            keys.append(jnp.concatenate([left, right], axis=1))
             x = lat[slot, b, :, 64:80, :].astype(F32)
+            roped = []
             for quad in range(0, N, 4):
                 lines = [
-                    jnp.concatenate([x[a][0:8, 32 * g : 32 * g + 32] for a in range(quad, quad + 4)], axis=1)
+                    jnp.concatenate([x[q][0:8, 32 * g : 32 * g + 32] for q in range(quad, quad + 4)], axis=1)
                     for g in range(4)
                 ]
                 roped.append(jnp.concatenate(lines, axis=0).astype(BF16))
-        keys = jnp.concatenate(
-            [jnp.concatenate(left, axis=0), jnp.concatenate(right, axis=0)], axis=1
-        )
-        ropes = jnp.concatenate(roped, axis=1)
-        scores = dot_t(q_lat[...], keys) + dot(q_rot[...], ropes)
-        j = lax.broadcasted_iota(jnp.int32, (1, 1024), 1)
-        slot = lax.shift_right_logical(j, 8)
-        a = lax.bitwise_and(lax.shift_right_logical(j, 5), 7)
-        r = lax.bitwise_and(j, 31)
-        block = jnp.where((slot == 0) | (slot == 3), b0 * N + a, a * N + b1)
-        which = jnp.where(slot < 2, 2 * parity + slot, 5 - 2 * parity - slot)
-        spots = block * ROWS + which * 32 + r
-        rows = lax.broadcasted_iota(jnp.int32, (3 * ROWS, 1), 0)
-        rows = sp * ROWS + lax.bitwise_and(rows, ROWS - 1)
-        scores = jnp.where(spots <= rows, scores, LOW)
-        old = top[:, 0:1]
-        new = jnp.maximum(old, jnp.max(scores, axis=1, keepdims=True))
-        weights = jnp.exp2(scores - new)
+            value = dot_t(q_lat[...], keys[-1]) + dot(q_rot[...], jnp.concatenate(roped, axis=1))
+            block = b * N + a if slot in (0, 3) else a * N + b
+            which = 2 * parity + slot if slot < 2 else 5 - 2 * parity - slot
+            value = jnp.where(block * ROWS + which * 32 + r <= rows, value, LOW)
+            new = jnp.maximum(new, jnp.max(value, axis=1, keepdims=True))
+            scores.append(value)
         shrink = jnp.exp2(old - new)
-        total[...] = total[...] * shrink + jnp.sum(weights, axis=1, keepdims=True)
-        acc[...] = acc[...] * shrink + dot(weights.astype(BF16), keys)
+        update = acc[...] * shrink
+        lanes = total[...] * shrink
+        for key, value in zip(keys, scores):
+            weights = jnp.exp2(value - new)
+            lanes = lanes + (weights[:, :128] + weights[:, 128:])
+            update = update + dot(weights.astype(BF16), key)
+        acc[...] = update
+        total[...] = lanes
         top[...] = jnp.broadcast_to(new, top.shape)
 
     stage("lat1")
@@ -352,29 +414,30 @@
     weight_step(1, True, True)
     stage("ring1a")
     lat_pass(1, 0, True, True)
+    stage("over0")
+    pass_over(0)
     stage("ring1b")
     lat_pass(1, 1, True, True)
     hand_over(wrap(beta + N - 1))
     hand_over(wrap(beta + 1))
-    stage("over0")
-    pass_over(0)
+    stage("w0")
+    wgt_pass(0, 0)
     stage("w1_2")
     weight_step(2, True, True)
-    stage("attend0")
-    attend(0)
     stage("ring2a")
     lat_pass(2, 0, True, True)
+    stage("over1")
+    pass_over(1)
     stage("ring2b")
     lat_pass(2, 1, True, True)
     hand_over(wrap(beta + N - 2))
     hand_over(wrap(beta + 2))
     stage("w1_3")
     weight_step(3, True, False)
-    stage("over1")
-    pass_over(1)
+    wgt_pass(0, 1)
+    attend(0)
     stage("over2")
     pass_over(2)
-    stage("attend1")
     attend(1)
     stage("ring3")
     lat_pass(3, 0, True, False)
@@ -383,10 +446,10 @@
     for k in (3, 4):
         a = wrap(alpha + k)
         arrived(wgt.at[beta, a], w1r.at[a])
-    wgt_pass(0, 0)
-    wgt_pass(0, 1)
-    stage("attend2")
-    attend(2)
+    wgt_pass(0, 2)
+    wgt_pass(0, 3)
+    stage("p1_0")
+    wgt_pass(1, 0)
     stage("ring3end")
     for b, p in ((wrap(beta + N - 3), 1), (wrap(beta + 3), 0)):
         arrived(lat_piece(b, p), l2r.at[2 * b + p])
@@ -394,49 +457,42 @@
     hand_over(wrap(beta + 3))
     stage("over3")
     pass_over(3)
-    wgt_pass(0, 2)
+    attend(2)
     stage("ring4")
     b = wrap(beta + 4)
     arrived(lat_piece(b, 0), l2r.at[2 * b])
     arrived(lat_piece(b, 1), l2r.at[2 * b + 1])
-    hand_over(b)
-    wgt_pass(0, 3)
+    hand_over(wrap(beta + 4))
     stage("over4")
     pass_over(4)
-    stage("attend3")
     attend(3)
-    stage("pass1_0")
-    wgt_pass(1, 0)
+    stage("p1_1")
+    wgt_pass(1, 1)
     stage("over5")
     pass_over(5)
-    stage("attend4")
     attend(4)
-    stage("pass1_1")
-    wgt_pass(1, 1)
+    stage("p1_2")
+    wgt_pass(1, 2)
     stage("over6")
     pass_over(6)
-    stage("attend5")
-    attend(5)
-    stage("pass1_2")
-    wgt_pass(1, 2)
     stage("over7")
     pass_over(7)
-    stage("attend6")
-    attend(6)
-    stage("pass1_3")
+    attend(5)
+    stage("p1_3")
     wgt_pass(1, 3)
-    stage("attend7")
-    attend(7)
-    stage("pass2_0")
+    attend(6, 7)
+    stage("p2_0")
     wgt_pass(2, 0)
+    stage("p2_1")
+    wgt_pass(2, 1)
     stage("heads")
-    normed = (acc[...] / total[:, 0:1]).astype(BF16)
+    normed = (acc[...] / jnp.sum(total[...], axis=1, keepdims=True)).astype(BF16)
     raw_a = jnp.concatenate(
         [dot(normed[h * ROWS : (h + 1) * ROWS], wa_val[:, h * DA : (h + 1) * DA]) for h in range(2)], axis=1
     )
     raw_b = dot(normed[2 * ROWS :], wb_val[...])
     power = jnp.sum(raw_a * raw_a, axis=1, keepdims=True) + jnp.sum(raw_b * raw_b, axis=1, keepdims=True)
-    energy[tp] = jnp.broadcast_to(power, (ROWS, ROWS)).T[0:8]
+    energy[4] = jnp.broadcast_to(power, (ROWS, ROWS)).T[0:8]
     gained = jnp.concatenate([raw_a * gain_a[...], raw_b * gain_b[...]], axis=1).astype(BF16)
     local[0].wait()
     local[1].wait()
@@ -444,28 +500,54 @@
     def of_tp(t):
         return pl.ds(pl.multiple_of(t * COLS, COLS), COLS)
 
-    stage("mixsend")
-    order = (4, 5, 3, 2, 6, 7, 1)
-    for k in order:
-        t = wrap(tp + k)
-        mix_out[t] = dot(gained, w_out[:, of_tp(t)]).astype(BF16)
-        send(mix_out.at[t], mix_in.at[tp], mxs.at[k], mxr.at[tp], along_tp(k))
-        send(energy.at[tp], energy.at[tp], ens.at[k], enr.at[tp], along_tp(k))
-    mix = dot(gained, w_out[:, of_tp(tp)])
-    stage("pass2_123")
-    wgt_pass(2, 1)
+    chip = lax.div(tp, 2)
+
+    def scattered(partial, leaving, paired, coming, pxs, pxr, ssem, rsem, between):
+        for k in (2, 1, 3, 0):
+            at = lax.rem(chip + k, 4)
+            t = 2 * at + 1 - core
+            leaving[t] = partial(t).astype(BF16)
+            send(leaving.at[t], paired.at[at], pxs.at[k], pxr.at[at], partner)
+        between()
+        for k in (2, 1, 3):
+            at = lax.rem(chip + k, 4)
+            t = 2 * at + core
+            value = partial(t)
+            arrived(paired.at[at], pxr.at[at])
+            leaving[t] = (value + paired[at].astype(F32)).astype(BF16)
+            send(leaving.at[t], coming.at[chip], ssem.at[k], rsem.at[chip], (sp, t))
+        value = partial(tp)
+        arrived(paired.at[chip], pxr.at[chip])
+        return value + paired[chip].astype(F32)
+
+    def collected(value, coming, rsem):
+        for k in (1, 3, 2):
+            at = lax.rem(chip + k, 4)
+            arrived(coming.at[at], rsem.at[at])
+            value = value + coming[at].astype(F32)
+        return value
+
+    def share_energy():
+        send(energy.at[4], energy.at[5], ens.at[0], enr.at[4], partner)
+
+    mix = scattered(
+        lambda t: dot(gained, w_out[:, of_tp(t)]), mix_out, mix_pair, mix_in, mps, mpr, mxs, mxr, share_energy
+    )
+    arrived(energy.at[5], enr.at[4])
+    energy[chip] = energy[4] + energy[5]
+    for k in (2, 1, 3):
+        to = (sp, wrap(tp + 2 * k))
+        send(energy.at[chip], energy.at[chip], ens.at[k], enr.at[chip], to)
+    stage("pass2_23")
     wgt_pass(2, 2)
     wgt_pass(2, 3)
     stage("mixwait")
-    for k in order:
-        t = wrap(tp + k)
-        arrived(mix_in.at[t], mxr.at[t])
-        arrived(energy.at[t], enr.at[t])
-        mix = mix + mix_in[t].astype(F32)
+    mix = collected(mix, mix_in, mxr)
+    for k in (1, 2, 3):
+        at = lax.rem(chip + k, 4)
+        arrived(energy.at[at], enr.at[at])
     stage("mixsum")
-    power = energy[0]
-    for t in range(1, N):
-        power = power + energy[t]
+    power = energy[0] + energy[1] + energy[2] + energy[3]
     factor = lax.rsqrt(power[0:1] / (HA * DA + HB * DB) + EPS_RMS)
     factor = jnp.broadcast_to(factor, (ROWS, ROWS)).T[:, 0:1]
     pre[tp] = (ALPHA * resid[...].astype(F32) + mix * factor).astype(BF16)
@@ -474,25 +556,31 @@
     send(pre.at[tp], pre.at[tp], prs.at[1], prr.at[tp], partner)
     for t in range(N):
         send(pre.at[tp, ROWS - HALO : ROWS], pre_halo.at[tp], hls.at[t], hlr.at[tp], (nxt[0], t))
-    stage("pass3")
+    stage("pass3a")
     wgt_pass(3, 0, True, False)
     wgt_pass(3, 2, False, True)
     wgt_pass(3, 1, True, False)
-    wgt_pass(3, 3, False, True)
     stage("prewait")
+    center_sum = {}
+
+    def note(t, key):
+        value = pre[t].astype(F32)
+        amount = jnp.sum(value, axis=1, keepdims=True)
+        shifted = value - amount / COLS
+        center_sum[key] = (amount, jnp.sum(shifted * shifted, axis=1, keepdims=True))
+
+    note(tp, 0)
     for k in (2, 6, 4):
         t = wrap(tp + k)
         arrived(pre.at[t], prr.at[t])
         send(pre.at[t], pre.at[t], prs.at[k + 1], prr.at[t], partner)
+        if k == 2:
+            wgt_pass(3, 3, False, True)
+        note(t, k)
     stage("halowait")
     for t in range(N):
         arrived(pre_halo.at[t], hlr.at[t])
-    stage("prewait2")
-    for k in (1, 3, 5, 7):
-        t = wrap(tp + k)
-        arrived(pre.at[t], prr.at[t])
-
-    stage("norm1")
+
     def row_stats(ref):
         middle = jnp.sum(ref[0].astype(F32), axis=1, keepdims=True)
         for t in range(1, N):
@@ -504,8 +592,20 @@
             wide = wide + jnp.sum(shifted * shifted, axis=1, keepdims=True)
         return middle, lax.rsqrt(wide / D + EPS_NORM)
 
-    center, scale = row_stats(pre)
     center_halo, scale_halo = row_stats(pre_halo)
+    stage("prewait2")
+    for k in (1, 3, 7, 5):
+        t = tp + 1 - 2 * core if k == 1 else wrap(tp + 1 - 2 * core + k - 1)
+        arrived(pre.at[t], prr.at[t])
+        note(t, k)
+
+    stage("norm1")
+    center = sum(amount for amount, _ in center_sum.values()) / D
+    wide = sum(apart for _, apart in center_sum.values())
+    for amount, _ in center_sum.values():
+        gap = amount / COLS - center
+        wide = wide + COLS * gap * gap
+    scale = lax.rsqrt(wide / D + EPS_NORM)
 
     def normed_cols(t):
         gain = norm1_gain[:, t * COLS : (t + 1) * COLS]
@@ -522,10 +622,11 @@
 
     @pl.when(core == 1)
     def _():
-        for t in range(N):
-            value = normed_cols(t)
+        for quad in range(0, N, 4):
+            values = [normed_cols(t) for t in range(quad, quad + 4)]
             for g in range(N):
-                first[:, g * COLS + t * 32 : g * COLS + (t + 1) * 32] = value[:, g * 32 : (g + 1) * 32]
+                at = g * COLS + quad * 32
+                first[:, at : at + 128] = jnp.concatenate([v[:, g * 32 : g * 32 + 32] for v in values], axis=1)
 
     def project(i):
         b = wrap(beta + offset(i))
@@ -583,17 +684,12 @@
 
     stage("down")
     local[2].wait()
-    for k in order:
-        t = wrap(tp + k)
-        down_out[t] = dot(hidden[...], w_down[:, of_tp(t)]).astype(BF16)
-        send(down_out.at[t], down_in.at[tp], dns.at[k], dnr.at[tp], along_tp(k))
-    value = dot(hidden[...], w_down[:, of_tp(tp)]) + ALPHA * first_own[...].astype(F32)
+    value = scattered(
+        lambda t: dot(hidden[...], w_down[:, of_tp(t)]), down_out, down_pair, down_in, dps, dpr, dns, dnr, lambda: None
+    )
+    value = value + ALPHA * first_own[...].astype(F32)
     stage("downwait")
-    for k in order:
-        t = wrap(tp + k)
-        arrived(down_in.at[t], dnr.at[t])
-        value = value + down_in[t].astype(F32)
-
+    value = collected(value, down_in, dnr)
     stage("stats")
     amount = jnp.sum(value, axis=1, keepdims=True)
     apart = value - amount / COLS
@@ -604,10 +700,10 @@
         jnp.broadcast_to(amount, (ROWS, ROWS)).T[0:8],
         jnp.broadcast_to(apart, (ROWS, ROWS)).T[0:8],
     )
-    for k in order:
+    for k in (4, 5, 3, 2, 6, 7, 1):
         send(stats.at[tp], stats.at[tp], sts.at[k], srr.at[tp], along_tp(k))
     stage("statswait")
-    for k in order:
+    for k in range(1, N):
         t = wrap(tp + k)
         arrived(stats.at[t], srr.at[t])
     stage("finish")
@@ -686,13 +782,12 @@
         ffn_down,
         norm2_gain[None],
     )
-    specs = [vmem] * len(operands)
-    for at in (15, 16, 22):
-        specs[at] = anywhere
+    specs = [anywhere] * len(operands)
+    small = [x for at, x in enumerate(operands) if at not in (15, 16, 22)]
     dma = pltpu.SemaphoreType.DMA
     return pl.pallas_call(
         kernel,
-        out_shape=jax.ShapeDtypeStruct((ROWS, COLS), BF16),
+        out_shape=pltpu.VMEM((ROWS, COLS), BF16),
         in_specs=specs,
         out_specs=vmem,
         scratch_shapes=[
@@ -706,7 +801,8 @@
             pltpu.VMEM((256, D), BF16),
             pltpu.VMEM((UNITS, D), BF16),
             pltpu.VMEM((N, ROWS, COLS), BF16),
-            pltpu.VMEM((N, ROWS, COLS), BF16),
+            pltpu.VMEM((4, ROWS, COLS), BF16),
+            pltpu.VMEM((4, ROWS, COLS), BF16),
             pltpu.VMEM((N, 8, ROWS), F32),
             pltpu.VMEM((N, ROWS, COLS), BF16),
             pltpu.VMEM((N, HALO, COLS), BF16),
@@ -715,7 +811,8 @@
             pltpu.VMEM((HALO + ROWS, 2 * UNITS), F32),
             pltpu.VMEM((ROWS, UNITS), BF16),
             pltpu.VMEM((N, ROWS, COLS), BF16),
-            pltpu.VMEM((N, ROWS, COLS), BF16),
+            pltpu.VMEM((4, ROWS, COLS), BF16),
+            pltpu.VMEM((4, ROWS, COLS), BF16),
             pltpu.VMEM((N, 8, ROWS), F32),
             dma((3,)),
             dma((7,)),
@@ -744,6 +841,12 @@
             dma((8,)),
             dma((8,)),
             dma((8,)),
+            dma((4,)),
+            dma((4,)),
+            dma((4,)),
+            dma((4,)),
+            dma((len(small),)),
+            *[pltpu.VMEM(x.shape, x.dtype) for x in small],
         ],
         compiler_params=pltpu.CompilerParams(
             collective_id=0, has_side_effects=True, vmem_limit_bytes=56 * 1024 * 1024

time: 86.1 us -> 80.2 us (0.931)
  Pallas kernels: 84.4 us -> 79.4 us
    pallas_call x1, Pallas kernels: 84.4 us -> 79.4 us  [shards(): pl.pallas_call(kernel, out_shape=pltpu.VMEM((ROWS, COLS), BF16), in_specs...]
where the time goes in v3:
time: 80.2 us; the launch traced here: 80.1 us
  Pallas kernels  79.4 us (99%)
    pallas_call x1, Pallas kernels, shards(): pl.pallas_call(kernel, out_shape=pltpu.VMEM((ROWS, COLS), BF16), in_specs...  79.4 us

profile of v3, /device:TPU:1, one launch (start us, length us, event | category | flops | bytes accessed | tf_op | source)
XLA Modules:
  0.0 80.1 jit_solution(9029498881189225775)
XLA Ops:
  0.0 79.4 %shard_map.226 = bf16[128,256]{1,0:T(8,128)(2,1)S(1)} custom-call(f32[16,128]{1,0:T(8,128)} %constant.2.clone.freq_hbm, bf16[128,256]{1,0:T(8,128)(2,1)} %resid_hbm.1, bf16[128,128]{1,0:T(8,128)(2,1)} %qa_nope_hbm.1, bf16[128,128]{1,0:T(8,128)(2,1)} %qb_nope_hbm.1, bf16[64,128]{1,0:T(8,128)(2,1)} %bitcast.8, bf16[32,128]{1,0:T(8,128)(2,1)} %bitcast.9, ...), custom_call_target="tpu_custom_call" | custom-call | flops 8000000000 | bytes 20000000 | tf_op jit(solution)/shard_map/pallas_call | solution.py:788
  79.4 0.6 copy.26

commit v4 on v3

--- a/solution.py
+++ b/solution.py
@@ -355,16 +355,19 @@
                 at = base + 4 * d + (p if d < 3 or k == 1 else p - 2)
                 send(wgt_piece(b, p), wgt_piece(b, p), w2s.at[at], w2r.at[4 * b + p], along_b(k))
 
-    def attend(*steps):
-        stage(f"attend{steps[-1]}")
+    def attend(near, *steps):
+        stage(f"{'near' if near else 'far'}{steps[-1]}")
         places = []
         for i in steps:
             b0 = wrap(z + offset(i))
             b1 = wrap(y + offset(i))
             theirs = wrap(alpha + offset(i))
-            arrived(lat.at[1 - core, theirs], ddr.at[theirs])
-            arrived(lat.at[2 + core, theirs], xdr.at[theirs])
-            places += [(0, b0), (1, b1), (2, b1), (3, b0)]
+            if near:
+                arrived(lat.at[1 - core, theirs], ddr.at[theirs])
+                places += [(0, b0), (1, b1)]
+            else:
+                arrived(lat.at[2 + core, theirs], xdr.at[theirs])
+                places += [(2, b1), (3, b0)]
         rows = lax.broadcasted_iota(jnp.int32, (3 * ROWS, 1), 0)
         rows = sp * ROWS + lax.bitwise_and(rows, ROWS - 1)
         j = lax.broadcasted_iota(jnp.int32, (1, 256), 1)
@@ -412,6 +415,7 @@
     hand_over(beta)
     stage("w1_1")
     weight_step(1, True, True)
+    attend(True, 0)
     stage("ring1a")
     lat_pass(1, 0, True, True)
     stage("over0")
@@ -424,6 +428,7 @@
     wgt_pass(0, 0)
     stage("w1_2")
     weight_step(2, True, True)
+    attend(False, 0)
     stage("ring2a")
     lat_pass(2, 0, True, True)
     stage("over1")
@@ -435,10 +440,9 @@
     stage("w1_3")
     weight_step(3, True, False)
     wgt_pass(0, 1)
-    attend(0)
+    attend(True, 1, 2)
     stage("over2")
     pass_over(2)
-    attend(1)
     stage("ring3")
     lat_pass(3, 0, True, False)
     lat_pass(3, 1, False, True)
@@ -457,32 +461,34 @@
     hand_over(wrap(beta + 3))
     stage("over3")
     pass_over(3)
-    attend(2)
+    attend(False, 1, 2)
+    stage("over4")
+    pass_over(4)
+    attend(True, 3, 4)
     stage("ring4")
     b = wrap(beta + 4)
     arrived(lat_piece(b, 0), l2r.at[2 * b])
     arrived(lat_piece(b, 1), l2r.at[2 * b + 1])
     hand_over(wrap(beta + 4))
-    stage("over4")
-    pass_over(4)
-    attend(3)
     stage("p1_1")
     wgt_pass(1, 1)
+    attend(True, 5, 6)
     stage("over5")
     pass_over(5)
-    attend(4)
+    attend(False, 3, 4)
     stage("p1_2")
     wgt_pass(1, 2)
     stage("over6")
     pass_over(6)
+    attend(True, 7)
+    stage("p1_3")
+    wgt_pass(1, 3)
     stage("over7")
     pass_over(7)
-    attend(5)
-    stage("p1_3")
-    wgt_pass(1, 3)
-    attend(6, 7)
+    attend(False, 5, 6)
     stage("p2_0")
     wgt_pass(2, 0)
+    attend(False, 7)
     stage("p2_1")
     wgt_pass(2, 1)
     stage("heads")

time: 80.2 us -> 79.5 us (level)
  no operation moved by 1% of the time
where the time goes in v4:
time: 79.5 us; the launch traced here: 79.3 us
  Pallas kernels  78.7 us (99%)
    pallas_call x1, Pallas kernels, shards(): pl.pallas_call(kernel, out_shape=pltpu.VMEM((ROWS, COLS), BF16), in_specs...  78.7 us

profile of v4, /device:TPU:1, one launch (start us, length us, event | category | flops | bytes accessed | tf_op | source)
XLA Modules:
  0.0 79.3 jit_solution(15737979589309696533)
XLA Ops:
  0.0 78.7 %shard_map.226 = bf16[128,256]{1,0:T(8,128)(2,1)S(1)} custom-call(f32[16,128]{1,0:T(8,128)} %constant.2.clone.freq_hbm, bf16[128,256]{1,0:T(8,128)(2,1)} %resid_hbm.1, bf16[128,128]{1,0:T(8,128)(2,1)} %qa_nope_hbm.1, bf16[128,128]{1,0:T(8,128)(2,1)} %qb_nope_hbm.1, bf16[64,128]{1,0:T(8,128)(2,1)} %bitcast.8, bf16[32,128]{1,0:T(8,128)(2,1)} %bitcast.9, ...), custom_call_target="tpu_custom_call" | custom-call | flops 8000000000 | bytes 20000000 | tf_op jit(solution)/shard_map/pallas_call | solution.py:794
  78.7 0.6 copy.26

commit v5 on v4

--- a/solution.py
+++ b/solution.py
@@ -447,11 +447,8 @@
     lat_pass(3, 0, True, False)
     lat_pass(3, 1, False, True)
     stage("w1_4")
-    for k in (3, 4):
-        a = wrap(alpha + k)
-        arrived(wgt.at[beta, a], w1r.at[a])
+    arrived(wgt.at[beta, wrap(alpha + 3)], w1r.at[wrap(alpha + 3)])
     wgt_pass(0, 2)
-    wgt_pass(0, 3)
     stage("p1_0")
     wgt_pass(1, 0)
     stage("ring3end")
@@ -461,6 +458,9 @@
     hand_over(wrap(beta + 3))
     stage("over3")
     pass_over(3)
+    stage("w1_5")
+    arrived(wgt.at[beta, wrap(alpha + 4)], w1r.at[wrap(alpha + 4)])
+    wgt_pass(0, 3)
     attend(False, 1, 2)
     stage("over4")
     pass_over(4)

time: 79.5 us -> 78.9 us (level)
  no operation moved by 1% of the time
where the time goes in v5:
time: 78.9 us; the launch traced here: 78.8 us
  Pallas kernels  78.1 us (99%)
    pallas_call x1, Pallas kernels, shards(): pl.pallas_call(kernel, out_shape=pltpu.VMEM((ROWS, COLS), BF16), in_specs...  78.1 us

profile of v5, /device:TPU:1, one launch (start us, length us, event | category | flops | bytes accessed | tf_op | source)
XLA Modules:
  0.0 78.8 jit_solution(18052574732680506295)
XLA Ops:
  0.0 78.1 %shard_map.226 = bf16[128,256]{1,0:T(8,128)(2,1)S(1)} custom-call(f32[16,128]{1,0:T(8,128)} %constant.2.clone.freq_hbm, bf16[128,256]{1,0:T(8,128)(2,1)} %resid_hbm.1, bf16[128,128]{1,0:T(8,128)(2,1)} %qa_nope_hbm.1, bf16[128,128]{1,0:T(8,128)(2,1)} %qb_nope_hbm.1, bf16[64,128]{1,0:T(8,128)(2,1)} %bitcast.8, bf16[32,128]{1,0:T(8,128)(2,1)} %bitcast.9, ...), custom_call_target="tpu_custom_call" | custom-call | flops 8000000000 | bytes 20000000 | tf_op jit(solution)/shard_map/pallas_call | solution.py:794
  78.1 0.6 copy.26
